TPU v7x, 32 devices: a whole 2x2x4 slice. The times are simulated.
32 devices in a mesh: fs: 8 (over z, y), tp: 4 (over x, core).
Axes of the slice: x: 2, y: 2, z: 4, core: 2. Of those that a mesh axis runs over, the one named last changes fastest.
Arguments:
- x_late: bfloat16 [6144, 2048], P(('fs', 'tp')), may hold values from -6 to 6
- x_early: bfloat16 [6144, 2048], P(('fs', 'tp')), may hold values from -6 to 6
- w_gate: bfloat16 [2048, 5632], P('fs', 'tp'), may hold values from -0.125 to 0.125
- w_value: bfloat16 [2048, 5632], P('fs', 'tp'), may hold values from -0.125 to 0.125
- conv_taps: float32 [3, 5632], P(None, 'tp'), may hold values from -3 to 3
- grad_hidden: bfloat16 [6144, 5632], P('fs', 'tp'), may hold values from -6 to 6
- sum_gate: float32 [2048, 5632], P('fs', 'tp'), may hold values from -6 to 6
- sum_value: float32 [2048, 5632], P('fs', 'tp'), may hold values from -6 to 6
- sum_taps: float32 [3, 5632], P(None, 'tp'), may hold values from -6 to 6
Outputs:
- hidden_late: bfloat16 [6144, 5632], P('fs', 'tp')
- grad_early: bfloat16 [6144, 2048], P(('fs', 'tp'))
- new_sum_gate: float32 [2048, 5632], P('fs', 'tp')
- new_sum_value: float32 [2048, 5632], P('fs', 'tp')
- new_sum_taps: float32 [3, 5632], P(None, 'tp')
All inputs are finite; a program needn't handle non-finite values.
Results may differ from a plain program's by a relative error of at most 0.015.
Values may be sent and summed in bfloat16 or wider, within the bound.
A program may use at most 128 MiB of HBM per device.

v0:
```python
import math
import functools

import jax
import jax.numpy as jnp
from jax import lax
from jax.experimental import pallas as pl
from jax.experimental.pallas import tpu as pltpu
from jax.sharding import PartitionSpec as P

root_half = 0.7071067811865476
density_norm = 0.3989422804014327


def causal_mix(gate_rows, taps):
    width = taps.shape[0]
    length = gate_rows.shape[0]
    padded = jnp.pad(gate_rows.astype(jnp.float32), ((width - 1, 0), (0, 0)))
    mixed_pre = jnp.zeros((length, gate_rows.shape[1]), jnp.float32)
    for j in range(width):
        mixed_pre = mixed_pre + padded[j : j + length] * taps[j]
    return (mixed_pre, padded)


def gelu_slope(mixed_pre):
    return (
        0.5 * (1.0 + lax.erf(mixed_pre * root_half))
        + mixed_pre * jnp.exp(-0.5 * mixed_pre * mixed_pre) * density_norm
    )


def back_mix(slope_rows, taps, padded):
    width = taps.shape[0]
    length = slope_rows.shape[0]
    grown = jnp.pad(slope_rows, ((0, width - 1), (0, 0)))
    d_gate = jnp.zeros(slope_rows.shape, jnp.float32)
    for j in range(width):
        d_gate = d_gate + grown[width - 1 - j : width - 1 - j + length] * taps[j]
    tap_terms = jnp.stack(
        [jnp.sum(slope_rows * padded[j : j + length], axis=0) for j in range(width)]
    )
    return (d_gate, tap_terms)


MESH = pl.DeviceIdType.MESH


def greet(n, me):
    barrier = pltpu.get_barrier_semaphore()
    for away in range(1, n):
        pl.semaphore_signal(
            barrier, inc=1, device_id={"fs": lax.rem(me + away, n)}, device_id_type=MESH
        )
    pl.semaphore_wait(barrier, n - 1)


def gather_kernel(n, *refs):
    mine, full = refs[:2], refs[2:4]
    up_out, up_in, down_out, down_in, y_out, y_in, cross_out, cross_in, own = refs[4:]
    rows = mine[0].shape[0]
    depth = n // 2
    me = lax.axis_index("fs")
    z, y = lax.div(me, 2), lax.rem(me, 2)
    even = lax.rem(z, 2) == 0
    mate = jnp.where(even, z + 1, z - 1)

    def slot(p, zz, yy):
        return full[p].at[pl.ds(pl.multiple_of((zz * 2 + yy) * rows, rows), rows)]

    def link(p, source, zz, yy, out_sem, in_sem, to_z, to_y):
        return pltpu.make_async_remote_copy(
            src_ref=source,
            dst_ref=slot(p, zz, yy),
            send_sem=out_sem,
            recv_sem=in_sem,
            device_id={"fs": to_z * 2 + to_y},
            device_id_type=MESH,
        )

    def up(p, k):
        source = mine[p] if k == 0 else slot(p, z - k, y)
        return link(p, source, z - k, y, up_out.at[p, k], up_in.at[p, k], z + 1, y)

    def down(p, k):
        source = mine[p] if k == 0 else slot(p, z + k, y)
        return link(p, source, z + k, y, down_out.at[p, k], down_in.at[p, k], z - 1, y)

    def over(p, j, zz):
        source = mine[p] if j == 0 else slot(p, zz, y)
        return link(p, source, zz, y, y_out.at[p, j], y_in.at[p, j], z, 1 - y)

    def arrived(p, zz, yy, out_sem, in_sem):
        return link(p, slot(p, zz, yy), zz, yy, out_sem, in_sem, z, 1 - y)

    def cross():
        return link(1, slot(1, z, 1 - y), z, 1 - y, cross_out, cross_in, mate, y)

    greet(n, me)
    for p in range(2):
        pl.when(z + 1 < depth)(lambda p=p: up(p, 0).start())
        pl.when(z > 0)(lambda p=p: down(p, 0).start())
    for p in (1, 0):
        over(p, 0, z).start()
    local = [pltpu.make_async_copy(mine[p], slot(p, z, y), own.at[p]) for p in range(2)]
    for copy in local:
        copy.start()

    def y_sent(p, k, upward):
        if k == 0 and p == 1:
            return even if upward else jnp.logical_not(even)
        return None

    for k in range(depth - 1):
        for p in range(2):

            @pl.when(z - 1 - k >= 0)
            def _():
                zz = z - 1 - k
                arrived(p, zz, y, up_out.at[p, k], up_in.at[p, k]).wait_recv()
                pl.when(z + 1 < depth)(lambda: up(p, k + 1).start())
                wanted = y_sent(p, k, True)
                send = lambda: over(p, 1 + 2 * k, zz).start()
                send() if wanted is None else pl.when(wanted)(send)

            @pl.when(z + 1 + k < depth)
            def _():
                zz = z + 1 + k
                arrived(p, zz, y, down_out.at[p, k], down_in.at[p, k]).wait_recv()
                pl.when(z > 0)(lambda: down(p, k + 1).start())
                wanted = y_sent(p, k, False)
                send = lambda: over(p, 2 + 2 * k, zz).start()
                send() if wanted is None else pl.when(wanted)(send)

        if k == 0:
            arrived(1, z, 1 - y, y_out.at[1, 0], y_in.at[1, 0]).wait_recv()
            cross().start()

    arrived(0, z, 1 - y, y_out.at[0, 0], y_in.at[0, 0]).wait_recv()
    for k in range(depth - 1):
        for p in range(2):

            @pl.when(z - 1 - k >= 0)
            def _():
                wanted = y_sent(p, k, True)
                take = lambda: arrived(
                    p, z - 1 - k, 1 - y, y_out.at[p, 1 + 2 * k], y_in.at[p, 1 + 2 * k]
                ).wait_recv()
                take() if wanted is None else pl.when(wanted)(take)

            @pl.when(z + 1 + k < depth)
            def _():
                wanted = y_sent(p, k, False)
                take = lambda: arrived(
                    p, z + 1 + k, 1 - y, y_out.at[p, 2 + 2 * k], y_in.at[p, 2 + 2 * k]
                ).wait_recv()
                take() if wanted is None else pl.when(wanted)(take)

    arrived(1, mate, 1 - y, cross_out, cross_in).wait_recv()
    cross().wait_send()
    for p in range(2):
        over(p, 0, z).wait_send()
        pl.when(z + 1 < depth)(lambda p=p: up(p, 0).wait_send())
        pl.when(z > 0)(lambda p=p: down(p, 0).wait_send())
        local[p].wait()
        for k in range(depth - 1):

            @pl.when(z - 1 - k >= 0)
            def _():
                pl.when(z + 1 < depth)(lambda: up(p, k + 1).wait_send())
                wanted = y_sent(p, k, True)
                end = lambda: over(p, 1 + 2 * k, z - 1 - k).wait_send()
                end() if wanted is None else pl.when(wanted)(end)

            @pl.when(z + 1 + k < depth)
            def _():
                pl.when(z > 0)(lambda: down(p, k + 1).wait_send())
                wanted = y_sent(p, k, False)
                end = lambda: over(p, 2 + 2 * k, z + 1 + k).wait_send()
                end() if wanted is None else pl.when(wanted)(end)


def gather_rows(w_gate, w_value):
    n = lax.axis_size("fs")
    depth = n // 2
    rows, columns = w_gate.shape
    sems = pltpu.SemaphoreType.DMA
    whole = jax.ShapeDtypeStruct((n * rows, columns), w_gate.dtype)
    hbm = pl.BlockSpec(memory_space=pl.ANY)
    return pl.pallas_call(
        functools.partial(gather_kernel, n),
        out_shape=(whole, whole),
        in_specs=[hbm, hbm],
        out_specs=(hbm, hbm),
        scratch_shapes=[
            sems((2, depth)),
            sems((2, depth)),
            sems((2, depth)),
            sems((2, depth)),
            sems((2, 2 * depth)),
            sems((2, 2 * depth)),
            sems,
            sems,
            sems((2,)),
        ],
        compiler_params=pltpu.CompilerParams(collective_id=0, has_side_effects=True),
        name="gather_rows",
    )(w_gate, w_value)


def scatter_kernel(n, factor, *refs):
    flipped, deltas, taps, rows_late = refs[0], refs[1:3], refs[3], refs[4]
    weights, conv = refs[5:7], refs[7]
    total, taps_total, hidden = refs[8:10], refs[10], refs[11]
    y_got, up_got, down_got, taps_got = refs[12:14], refs[14:16], refs[16:18], refs[18]
    cross_got, strip, terms = refs[19], refs[20], refs[21:23]
    y_out, y_in, z_out, up_in, down_in, taps_out, taps_in = refs[23:30]
    cross_out, cross_in, strip_in = refs[30:]
    rows = total[0].shape[0]
    depth = n // 2
    step = math.gcd(rows, 32)
    me = lax.axis_index("fs")
    z, y = lax.div(me, 2), lax.rem(me, 2)
    even = lax.rem(z, 2) == 0
    odd = jnp.logical_not(even)
    mate = jnp.where(even, z + 1, z - 1)
    lane = 128
    strips = hidden.shape[1] // lane

    def fetch(b):
        at = pl.ds(pl.multiple_of(b * lane, lane), lane)
        slot = lax.rem(b, 2)
        return [
            pltpu.make_async_copy(
                weights[i].at[:, at],
                strip.at[slot, :, pl.ds(i * lane, lane)],
                strip_in.at[slot, i],
            )
            for i in range(2)
        ]

    def late(first, last):
        def body(b, _):
            for copy in fetch(b):
                copy.wait()

            @pl.when(b + 1 < strips)
            def _():
                for copy in fetch(b + 1):
                    copy.start()

            at = pl.ds(pl.multiple_of(b * lane, lane), lane)
            both = jnp.dot(
                rows_late[...], strip[lax.rem(b, 2)], preferred_element_type=jnp.float32
            )
            both = both.astype(jnp.bfloat16).astype(jnp.float32)
            gate = both[:, :lane]
            width = conv.shape[0]
            position = lax.broadcasted_iota(jnp.int32, gate.shape, 0)
            pre = gate * conv[pl.ds(width - 1, 1), at]
            for j in range(width - 1):
                lag = width - 1 - j
                moved = jnp.where(position >= lag, pltpu.roll(gate, lag, 0), 0.0)
                pre = pre + moved * conv[pl.ds(j, 1), at]
            active = 0.5 * pre * (1.0 + lax.erf(pre * root_half))
            hidden[:, at] = (active * both[:, lane:]).astype(hidden.dtype)
            return 0

        lax.fori_loop(first, last, body, 0)

    def start_of(zz, yy):
        return pl.multiple_of((zz * 2 + yy) * rows, rows)

    def make(p, zz, yy):
        at = pl.ds(start_of(zz, yy), rows)
        term = jnp.dot(flipped[at, :], deltas[p][...], preferred_element_type=jnp.float32)
        terms[p][at, :] = (factor * term).astype(terms[p].dtype)

    def over(p, zz, source=None):
        return pltpu.make_async_remote_copy(
            src_ref=terms[p].at[pl.ds(start_of(zz, 1 - y), rows)] if source is None else source,
            dst_ref=y_got[p].at[zz],
            send_sem=y_out.at[p, zz],
            recv_sem=y_in.at[p, zz],
            device_id={"fs": z * 2 + 1 - y},
            device_id_type=MESH,
        )

    def along(p, zz, away, upward):
        got, sem = (up_got, up_in) if upward else (down_got, down_in)
        return pltpu.make_async_remote_copy(
            src_ref=y_got[p].at[zz],
            dst_ref=got[p].at[away - 1],
            send_sem=z_out.at[p, zz],
            recv_sem=sem.at[p, away - 1],
            device_id={"fs": (z + 1 if upward else z - 1) * 2 + y},
            device_id_type=MESH,
        )

    def cross():
        return pltpu.make_async_remote_copy(
            src_ref=terms[1].at[pl.ds(start_of(mate, 1 - y), rows)],
            dst_ref=cross_got,
            send_sem=cross_out,
            recv_sem=cross_in,
            device_id={"fs": mate * 2 + y},
            device_id_type=MESH,
        )

    def add_cross():
        base = start_of(z, 1 - y)

        def body(i, _):
            part = pl.ds(pl.multiple_of(i * step, step), step)
            value = terms[1][pl.ds(pl.multiple_of(base + i * step, step), step), :]
            value = value.astype(jnp.float32) + cross_got[part, :].astype(jnp.float32)
            cross_got[part, :] = value.astype(cross_got.dtype)
            return 0

        lax.fori_loop(0, rows // step, body, 0)

    def over_y(p, away, upward):
        if p == 1 and away == 1:
            return odd if upward else even
        return True

    def taps_copy(away):
        return pltpu.make_async_remote_copy(
            src_ref=taps,
            dst_ref=taps_got.at[me],
            send_sem=taps_out.at[away],
            recv_sem=taps_in.at[me],
            device_id={"fs": lax.rem(me + away, n)},
            device_id_type=MESH,
        )

    def add(p, zz, others, into, from_y=True):
        base = start_of(zz, y)

        def body(i, _):
            part = pl.ds(pl.multiple_of(i * step, step), step)
            value = terms[p][
                pl.ds(pl.multiple_of(base + i * step, step), step), :
            ].astype(jnp.float32)
            if from_y:
                value = value + y_got[p][zz, part, :].astype(jnp.float32)
            for ref, at in others:
                value = value + ref[at, part, :].astype(jnp.float32)
            if into is None:
                y_got[p][zz, part, :] = value.astype(y_got[p].dtype)
            else:
                into[part, :] = value.astype(into.dtype)
            return 0

        lax.fori_loop(0, rows // step, body, 0)

    for copy in fetch(0):
        copy.start()
    greet(n, me)
    make(1, mate, 1 - y)
    cross().start()

    def send_terms(i, _):
        away = depth - 1 - i
        for p in range(2):
            up_too = z + away < depth
            down_too = z - away >= 0
            if p == 1:
                up_too = jnp.logical_and(up_too, jnp.logical_or(away > 1, odd))
                down_too = jnp.logical_and(down_too, jnp.logical_or(away > 1, even))
            for here, zz in ((up_too, z + away), (down_too, z - away)):

                @pl.when(here)
                def _():
                    make(p, zz, 1 - y)
                    over(p, zz).start()

        return 0

    lax.fori_loop(0, depth - 1, send_terms, 0)
    make(0, z, 1 - y)
    over(0, z).start()
    for away in range(1, n):
        taps_copy(away).start()

    def pass_on(p, away, upward):
        zz = z + away if upward else z - away
        inside = zz < depth if upward else zz >= 0
        has_more = z > 0 if upward else z + 1 < depth
        got = up_got if upward else down_got
        kinds = [(True, True)]
        if p == 1 and away == 1:
            kinds = [(True, odd if upward else even), (False, even if upward else odd)]

        @pl.when(inside)
        def _():
            if away < depth - 1:
                pl.when(has_more)(lambda: along(p, zz, away + 1, upward).wait_recv())
            for from_y, here in kinds:

                @pl.when(jnp.logical_and(inside, here))
                def _():
                    if from_y:
                        over(p, zz).wait_recv()

                    @pl.when(has_more)
                    def _():
                        add(p, zz, [(got[p], away)] if away < depth - 1 else [], None, from_y)

                    @pl.when(jnp.logical_not(has_more))
                    def _():
                        add(p, zz, [], None, from_y)

            along(p, zz, away, upward).start()

    make(1, z, 1 - y)

    def own_terms(zz, _):
        for p in range(2):
            make(p, zz, y)
        return 0

    lax.fori_loop(0, depth, own_terms, 0)
    done = min(1, strips)
    late(0, done)
    for away in range(depth - 1, 0, -1):
        for p in range(2):
            pass_on(p, away, True)
            pass_on(p, away, False)
            if away == depth - 1 and p == 1:
                cross().wait_recv()
                add_cross()
                over(1, z, cross_got).start()
            if done < strips:
                upto = min(done + 2, strips)
                late(done, upto)
                done = upto
    if done < strips:
        late(done, strips)

    taps_got[pl.ds(me, 1)] = taps[...][None]
    for away in range(1, n):
        source = lax.rem(me + away, n)
        pltpu.make_async_remote_copy(
            src_ref=taps,
            dst_ref=taps_got.at[source],
            send_sem=taps_out.at[away],
            recv_sem=taps_in.at[source],
            device_id={"fs": source},
            device_id_type=MESH,
        ).wait_recv()
    sum_of = taps_got[0]
    for i in range(1, n):
        sum_of = sum_of + taps_got[i]
    taps_total[...] = sum_of

    for p in range(2):
        over(p, z).wait_recv()
        pl.when(z > 0)(lambda: along(p, z, 1, True).wait_recv())
        pl.when(z + 1 < depth)(lambda: along(p, z, 1, False).wait_recv())
        at_low, at_high = z == 0, z + 1 == depth
        both = jnp.logical_not(jnp.logical_or(at_low, at_high))
        pl.when(at_low)(lambda: add(p, z, [(down_got[p], 0)], total[p]))
        pl.when(at_high)(lambda: add(p, z, [(up_got[p], 0)], total[p]))
        pl.when(both)(lambda: add(p, z, [(up_got[p], 0), (down_got[p], 0)], total[p]))

    cross().wait_send()
    over(0, z).wait_send()
    over(1, z, cross_got).wait_send()
    for p in range(2):
        for away in range(depth - 1, 0, -1):
            up_too, down_too = over_y(p, away, True), over_y(p, away, False)

            @pl.when(z + away < depth)
            def _():
                pl.when(jnp.logical_and(z + away < depth, up_too))(
                    lambda: over(p, z + away).wait_send()
                )
                along(p, z + away, away, True).wait_send()

            @pl.when(z - away >= 0)
            def _():
                pl.when(jnp.logical_and(z - away >= 0, down_too))(
                    lambda: over(p, z - away).wait_send()
                )
                along(p, z - away, away, False).wait_send()

    for away in range(1, n):
        taps_copy(away).wait_send()


def scatter_rows(factor, flipped, d_gate, d_value, tap_terms, rows_late, gate_full, value_full, conv_taps):
    n = lax.axis_size("fs")
    depth = n // 2
    rows, columns = flipped.shape[0] // n, d_gate.shape[1]
    sems = pltpu.SemaphoreType.DMA
    vmem = pl.BlockSpec(memory_space=pltpu.VMEM)
    total = jax.ShapeDtypeStruct((rows, columns), jnp.float32)
    row_block = lambda count: pltpu.VMEM((count, rows, columns), d_gate.dtype)
    return pl.pallas_call(
        functools.partial(scatter_kernel, n, factor),
        out_shape=(
            total,
            total,
            jax.ShapeDtypeStruct(tap_terms.shape, jnp.float32),
            jax.ShapeDtypeStruct((rows_late.shape[0], columns), jnp.bfloat16),
        ),
        in_specs=[vmem] * 5 + [pl.BlockSpec(memory_space=pl.ANY)] * 2 + [vmem],
        out_specs=(vmem,) * 4,
        scratch_shapes=[row_block(depth)] * 2
        + [row_block(depth - 1)] * 4
        + [
            pltpu.VMEM((n,) + tap_terms.shape, jnp.float32),
            pltpu.VMEM((rows, columns), d_gate.dtype),
            pltpu.VMEM((2, gate_full.shape[0], 256), gate_full.dtype),
            pltpu.VMEM((n * rows, columns), d_gate.dtype),
            pltpu.VMEM((n * rows, columns), d_gate.dtype),
            sems((2, depth)),
            sems((2, depth)),
            sems((2, depth)),
            sems((2, depth)),
            sems((2, depth)),
            sems((n,)),
            sems((n,)),
            sems,
            sems,
            sems((2, 2)),
        ],
        compiler_params=pltpu.CompilerParams(
            collective_id=1, has_side_effects=True, vmem_limit_bytes=60 * 1024 * 1024
        ),
        name="scatter_rows",
    )(flipped, d_gate, d_value, tap_terms, rows_late, gate_full, value_full, conv_taps)


def shards(x_late, x_early, w_gate, w_value, conv_taps, grad_hidden, sum_gate, sum_value, sum_taps):
    columns = w_gate.shape[1]
    factor = 1.0 / math.sqrt(x_late.shape[0] * lax.axis_size("fs") * lax.axis_size("tp"))
    gate_full, value_full = gather_rows(w_gate, w_value)
    block_rows = lax.all_gather(x_late, "tp", axis=0, tiled=True)
    gathered = lax.all_gather(x_early, "tp", axis=0, tiled=True)
    gate_rows = jnp.dot(gathered, gate_full, preferred_element_type=jnp.float32).astype(
        jnp.bfloat16
    )
    value_rows = jnp.dot(gathered, value_full, preferred_element_type=jnp.float32).astype(
        jnp.bfloat16
    )
    mixed_pre, padded = causal_mix(gate_rows, conv_taps)
    upstream = grad_hidden.astype(jnp.float32)
    slope_rows = upstream * value_rows.astype(jnp.float32) * gelu_slope(mixed_pre)
    d_gate_f, tap_terms = back_mix(slope_rows, conv_taps, padded)
    d_gate = d_gate_f.astype(jnp.bfloat16)
    d_value = (upstream * jax.nn.gelu(mixed_pre, approximate=False)).astype(jnp.bfloat16)
    contract = (((1,), (1,)), ((), ()))
    grad_early = lax.psum_scatter(
        (
            lax.dot_general(d_gate, gate_full, contract, preferred_element_type=jnp.float32)
            + lax.dot_general(d_value, value_full, contract, preferred_element_type=jnp.float32)
        ).astype(jnp.bfloat16),
        "tp",
        scatter_dimension=0,
        tiled=True,
    )
    taps_padded = jnp.pad(factor * tap_terms, ((0, -tap_terms.shape[0] % 8), (0, 0)))
    gate_total, value_total, tap_total, hidden = scatter_rows(
        factor,
        gathered.T,
        d_gate,
        d_value,
        taps_padded,
        block_rows,
        gate_full,
        value_full,
        conv_taps,
    )
    tap_total = tap_total[: tap_terms.shape[0]]
    return (
        hidden,
        grad_early,
        sum_gate + gate_total,
        sum_value + value_total,
        sum_taps + tap_total,
    )


def solution(mesh):
    placed = (
        P(("fs", "tp"), None),
        P(("fs", "tp"), None),
        P("fs", "tp"),
        P("fs", "tp"),
        P(None, "tp"),
        P("fs", "tp"),
        P("fs", "tp"),
        P("fs", "tp"),
        P(None, "tp"),
    )
    return jax.shard_map(
        shards,
        mesh=mesh,
        in_specs=placed,
        out_specs=(
            P("fs", "tp"),
            P(("fs", "tp"), None),
            P("fs", "tp"),
            P("fs", "tp"),
            P(None, "tp"),
        ),
        check_vma=False,
    )
```

profile of v0, /device:TPU:1, one launch (start us, length us, event | category | flops | bytes accessed | tf_op | source)
XLA Modules:
  0.0 319.7 jit_solution(6098155083773097308)
XLA Ops:
  7.2 0.0 all-gather.3.cloned.1.call-start
  7.2 0.7 all-gather.3.cloned.1.call-update
  7.9 0.0 all-gather.5.cloned.1.call-start
  7.9 0.7 all-gather.5.cloned.1.call-update
  8.6 0.0 reduce-scatter.2.cloned.1.call-start
  8.7 0.9 slice_reduce_fusion.2
  9.6 130.2 %gather_rows.1 = (bf16[2048,1408]{1,0:T(8,128)(2,1)}, bf16[2048,1408]{1,0:T(8,128)(2,1)}) custom-call(bf16[256,1408]{1,0:T(8,128)(2,1)} %refs_0_.1, bf16[256,1408]{1,0:T(8,128)(2,1)} %refs_1_.1), custom_call_target="tpu_custom_call" | custom-call | tf_op jit(solution)/shard_map/gather_rows/pallas_call | solution.py:189
  139.8 0.0 all-gather.3.cloned.1.call-done
  139.9 0.0 copy-start.6
  139.9 0.0 copy-start.3
  139.9 8.6 %convert_bitcast_fusion = f32[768,1408]{1,0:T(8,128)S(1)} fusion(bf16[768,2048]{1,0:T(8,128)(2,1)} %all-gather.3.cloned.1.call-done, bf16[2048,1408]{1,0:T(8,128)(2,1)} %get-tuple-element.12.refs_5_), kind=kOutput, calls=%fused_computation.13 | convolution fusion | flops 4431347712 | bytes 13238272 | tf_op jit(solution)/shard_map/dot_general | solution.py:541
  148.4 0.0 copy-done.6
  148.4 0.0 copy-start.2
  148.5 0.0 slice-start
  148.5 10.9 %fusion.1 = (bf16[768,1408]{1,0:T(8,128)(2,1)S(1)}, f32[768,1408]{1,0:T(8,128)S(1)}) fusion(bf16[768,1408]{1,0:T(8,128)(2,1)S(1)} %copy-done.6, f32[768,1408]{1,0:T(8,128)S(1)} %convert_bitcast_fusion, f32[1408]{0:T(1024)S(1)} %get-tuple-element.22, f32[1408]{0:T(1024)S(1)} %get-tuple-element.21, f32[1408]{0:T(1024)S(1)} %get-tuple-element.20), kind=kLoop, calls=%fused_computation.6 | loop fusion | flops 77856768 | bytes 12993024 | tf_op jit(solution)/shard_map/convert_element_type | solution.py:552
  159.4 0.0 copy-start
  159.4 0.0 copy-done.3
  159.4 0.0 copy-done.2
  159.4 0.0 slice-start.1
  159.4 6.1 %fusion = f32[768,1408]{1,0:T(8,128)S(1)} fusion(bf16[768,1408]{1,0:T(8,128)(2,1)S(1)} %copy-done.6, f32[768,1408]{1,0:T(8,128)S(1)} %get-tuple-element.24, bf16[768,2048]{1,0:T(8,128)(2,1)S(1)} %copy-done.3, bf16[2048,1408]{1,0:T(8,128)(2,1)S(1)} %copy-done.2), kind=kOutput, calls=%fused_computation.5 | convolution fusion | flops 4443242496 | bytes 19726336 | tf_op jit(solution)/shard_map/dot_general | solution.py:544
  165.5 3.2 multiply_reduce_fusion.2
  168.7 0.0 copy-start.1
  168.7 0.0 slice-done
  168.7 0.0 slice-done.1
  168.7 5.1 %fusion.15 = f32[768,2048]{1,0:T(8,128)S(1)} fusion(bf16[768,1408]{1,0:T(8,128)(2,1)S(1)} %get-tuple-element.25.refs_1_, bf16[2048,1408]{1,0:T(8,128)(2,1)S(1)} %bitcast.15), kind=kOutput, calls=%fused_computation.43 | convolution fusion | flops 4429185024 | bytes 14221312 | tf_op jit(solution)/shard_map/dot_general | solution.py:556
  173.8 0.0 copy-done.1
  173.8 0.0 copy-done
  173.8 6.6 %add_convert_fusion = bf16[768,2048]{1,0:T(8,128)(2,1)} fusion(f32[768,2048]{1,0:T(8,128)S(1)} %fusion.15, bf16[768,1408]{1,0:T(8,128)(2,1)S(1)} %get-tuple-element.23.refs_2_, bf16[2048,1408]{1,0:T(8,128)(2,1)S(1)} %copy-done.2), kind=kOutput, calls=%fused_computation.2 | convolution fusion | flops 4432330752 | bytes 17367040 | tf_op jit(solution)/shard_map/dot_general | solution.py:557
  180.4 0.0 copy-start.4
  180.4 0.0 reduce-scatter.2.cloned.1.call-update
  180.5 0.6 pad.14.refs_3_
  181.1 1.2 copy-done.4
  182.3 2.8 copy.15
  185.2 121.5 %scatter_rows.1 = (f32[256,1408]{1,0:T(8,128)}, f32[256,1408]{1,0:T(8,128)}, f32[8,1408]{1,0:T(8,128)}, bf16[768,1408]{1,0:T(8,128)(2,1)}) custom-call(bf16[2048,768]{1,0:T(8,128)(2,1)} %bitcast.13, bf16[768,1408]{1,0:T(8,128)(2,1)} %copy-done.1, bf16[768,1408]{1,0:T(8,128)(2,1)} %copy-done, f32[8,1408]{1,0:T(8,128)} %pad.14.refs_3_, ...), custom_call_target="tpu_custom_call" | custom-call | tf_op jit(solution)/shard_map/scatter_rows/pallas_call | solution.py:499
  306.7 0.0 copy-start.7
  306.7 0.0 copy-start.8
  306.7 0.0 copy-start.9
  306.7 0.0 copy-start.10
  306.8 0.0 copy-start.5
  306.8 3.2 add.45
  310.0 0.0 copy-done.7
  310.0 0.0 copy-done.8
  310.0 1.2 add.46
  311.2 0.0 copy-done.9
  311.2 0.0 copy-done.10
  311.2 0.6 slice_add_fusion
  311.8 0.0 copy-done.5
  311.8 1.3 copy.17
  (7 shorter events, 0.0 us)
Async XLA Ops:
  7.2 132.7 %all-gather.3.cloned.1.call-start = ((), (), s32[]{:S(2)}) async-start(), calls=%async_computation.1 | async-start | bytes 3932160 | tf_op jit(solution)/shard_map/all_gather | solution.py:540
  7.9 177.3 %all-gather.5.cloned.1.call-start = ((), (), s32[]{:S(2)}) async-start(), calls=%async_computation.2 | async-start | bytes 3932160 | tf_op jit(solution)/shard_map/all_gather | solution.py:539
  8.6 303.2 %reduce-scatter.2.cloned.1.call-start = ((), (), s32[]{:S(2)}) async-start(), calls=%async_computation.3 | async-start | bytes 3932160 | tf_op jit(solution)/shard_map/reduce_scatter | solution.py:554
  139.9 8.6 %copy-start.6 = (bf16[768,1408]{1,0:T(8,128)(2,1)S(1)}, bf16[768,1408]{1,0:T(8,128)(2,1)}, u32[]{:S(2)}) copy-start(bf16[768,1408]{1,0:T(8,128)(2,1)} %param.14) | copy-start | bytes 6488068
  139.9 19.5 %copy-start.3 = (bf16[768,2048]{1,0:T(8,128)(2,1)S(1)}, bf16[768,2048]{1,0:T(8,128)(2,1)}, u32[]{:S(2)}) copy-start(bf16[768,2048]{1,0:T(8,128)(2,1)} %all-gather.3.cloned.1.call-done) | copy-start | bytes 9437188
  148.4 10.9 %copy-start.2 = (bf16[2048,1408]{1,0:T(8,128)(2,1)S(1)}, bf16[2048,1408]{1,0:T(8,128)(2,1)}, u32[]{:S(2)}) copy-start(bf16[2048,1408]{1,0:T(8,128)(2,1)} %get-tuple-element.11.refs_6_) | copy-start | bytes 17301508
  148.5 20.3 %slice-start = ((s8[5767168]{0:T(1024)(128)(4,1)}), s8[4194304]{0:T(1024)(128)(4,1)S(1)}, s32[]{:S(2)}) async-start(s8[5767168]{0:T(1024)(128)(4,1)} %bitcast.14), calls=%async_computation.4 | async-start | bytes 8388608
  159.4 14.4 %copy-start = (bf16[768,1408]{1,0:T(8,128)(2,1)}, bf16[768,1408]{1,0:T(8,128)(2,1)S(1)}, u32[]{:S(2)}) copy-start(bf16[768,1408]{1,0:T(8,128)(2,1)S(1)} %get-tuple-element.23.refs_2_) | copy-start | bytes 6488068
  159.4 9.3 %slice-start.1 = ((s8[5767168]{0:T(1024)(128)(4,1)}), s8[1572864]{0:T(1024)(128)(4,1)S(1)}, s32[]{:S(2)}) async-start(s8[5767168]{0:T(1024)(128)(4,1)} %bitcast.14), calls=%async_computation.5 | async-start | bytes 3145728
  168.7 5.1 %copy-start.1 = (bf16[768,1408]{1,0:T(8,128)(2,1)}, bf16[768,1408]{1,0:T(8,128)(2,1)S(1)}, u32[]{:S(2)}) copy-start(bf16[768,1408]{1,0:T(8,128)(2,1)S(1)} %get-tuple-element.25.refs_1_) | copy-start | bytes 6488068
  180.4 1.9 copy-start.4
  306.7 3.2 %copy-start.7 = (f32[256,1408]{1,0:T(8,128)S(1)}, f32[256,1408]{1,0:T(8,128)}, u32[]{:S(2)}) copy-start(f32[256,1408]{1,0:T(8,128)} %param.16) | copy-start | bytes 4325380
  306.7 3.2 %copy-start.8 = (f32[256,1408]{1,0:T(8,128)S(1)}, f32[256,1408]{1,0:T(8,128)}, u32[]{:S(2)}) copy-start(f32[256,1408]{1,0:T(8,128)} %get-tuple-element.15) | copy-start | bytes 4325380
  306.7 4.5 %copy-start.9 = (f32[3,1408]{1,0:T(4,128)S(1)}, f32[3,1408]{1,0:T(4,128)}, u32[]{:S(2)}) copy-start(f32[3,1408]{1,0:T(4,128)} %param.17) | copy-start | bytes 50692
  306.7 4.5 %copy-start.10 = (f32[8,1408]{1,0:T(8,128)S(1)}, f32[8,1408]{1,0:T(8,128)}, u32[]{:S(2)}) copy-start(f32[8,1408]{1,0:T(8,128)} %get-tuple-element.16) | copy-start | bytes 135172
  306.8 5.1 %copy-start.5 = (bf16[768,1408]{1,0:T(8,128)(2,1)S(1)}, bf16[768,1408]{1,0:T(8,128)(2,1)}, u32[]{:S(2)}) copy-start(bf16[768,1408]{1,0:T(8,128)(2,1)} %get-tuple-element.31) | copy-start | bytes 6488068
Sparse Core Ops, SparseCore 0:
  9.5 30.9 all-gather.2
  42.1 28.4 all-gather.4
  180.6 38.1 reduce-scatter.1
where the time goes:
time: 324 us; the launch traced here: 320 us
  Pallas kernels  252 us (78%)
  matrix products  26.3 us (8%)
  other arithmetic  19.1 us (6%)
  between operations  14 us (4%)
  local copies, waits for them, and re-layouts  6.95 us (2%)
    pallas_call x1, Pallas kernels, gather_rows(): pl.pallas_call(functools.partial(gather_kernel, n), out_shape=(whole, who...  130 us
    pallas_call x1, Pallas kernels, scatter_rows(): pl.pallas_call(functools.partial(scatter_kernel, n, factor), out_shape=(t...  122 us
    convert_element_type x1, other arithmetic, shards(): (upstream * jax.nn.gelu(mixed_pre, approximate=False)).astype(jnp.bfloat16)  10.9 us
    dot_general x1, matrix products, shards(): jnp.dot(gathered, gate_full, preferred_element_type=jnp.float32)  8.55 us
    dot_general x1, matrix products, shards(): lax.dot_general(d_value, value_full, contract, preferred_element_type=jnp...  6.59 us
  transfers between devices with their start and end apart: 3, of which 0 were waited for; matrix products, arithmetic and copies ran while one was open for 16% of the time, Pallas kernels for 79%

commit v1 on v0

v1 whole, which is shorter than its diff:
```python
import functools
import math

import jax
import jax.numpy as jnp
from jax import lax
from jax.experimental import pallas as pl
from jax.experimental.pallas import tpu as pltpu
from jax.sharding import PartitionSpec as P

root_half = 0.7071067811865476
density_norm = 0.3989422804014327
MESH = pl.DeviceIdType.MESH
LANE = 128
LEAD = 2


def kernel(n, tp_n, factor, *refs):
    x_late, x_early, w_gate, w_value, conv, grad_hidden = refs[:6]
    hidden, grad_early, gate_total, value_total, taps_total = refs[6:11]
    (
        strip, late_rows, early_rows, flipped, cots, upstream, out_stage, wire, part_got,
        up_got, down_got, fin_got, partial, partial_got, taps_own, taps_got, conv_got,
    ) = refs[11:28]
    (
        w_out, w_in, up_out, up_in, down_out, down_in, share_out, share_in, u_out, u_in,
        h_out, h_in, q_out, q_in, z_out, zup_in, zdown_in, f_out, f_in, late_out, late_in,
        early_out, early_in, p_out, p_in, t_out, t_in, c_out, c_in,
    ) = refs[28:]
    depth, half = n // 2, tp_n // 2
    rows = gate_total.shape[0]
    columns = gate_total.shape[1]
    strips = columns // LANE
    tokens, width = early_rows.shape
    piece = x_early.shape[0]
    taps_count = conv.shape[0]
    lag = depth + LEAD
    me, tp = lax.axis_index("fs"), lax.axis_index("tp")
    z, y = lax.div(me, 2), lax.rem(me, 2)
    x, c = lax.div(tp, 2), lax.rem(tp, 2)
    same = c == y
    other = jnp.logical_not(same)
    role_fs, role_tp = z * 2 + c, x * 2 + y
    twin = {"fs": role_fs, "tp": role_tp}
    partner = {"fs": me, "tp": x * 2 + 1 - c}
    above, below = {"fs": me + 2, "tp": tp}, {"fs": me - 2, "tp": tp}
    has_up, has_down = z + 1 < depth, z > 0

    def send(src, dst, out_sem, in_sem, to):
        return pltpu.make_async_remote_copy(
            src_ref=src, dst_ref=dst, send_sem=out_sem, recv_sem=in_sem,
            device_id=to, device_id_type=MESH,
        )

    def landed(dst, sem):
        pltpu.make_async_copy(dst, dst, sem).wait()

    def lanes(s):
        return pl.ds(pl.multiple_of(s * LANE, LANE), LANE)

    def block(zz, cc):
        return pl.ds(pl.multiple_of((zz * 2 + cc) * rows, rows), rows)

    def own_slot(s, zz, cc):
        return strip.at[s, block(zz, cc)]

    barrier = pltpu.get_barrier_semaphore()

    def hail(i, _):
        j = lax.rem(me * 2 + c + i, 2 * n)
        pl.semaphore_signal(
            barrier, inc=1, device_id={"fs": lax.div(j, 2), "tp": x * 2 + lax.rem(j, 2)},
            device_id_type=MESH,
        )
        return 0

    lax.fori_loop(1, 2 * n, hail, 0)
    for dx in range(1, half):
        for yy in range(2):
            for cc in range(2):
                pl.semaphore_signal(
                    barrier, inc=1,
                    device_id={"fs": z * 2 + yy, "tp": lax.rem(x + dx, half) * 2 + cc},
                    device_id_type=MESH,
                )
    pl.semaphore_wait(barrier, 2 * n - 1 + 4 * (half - 1))

    def weights_away(s, there):
        for source, at in ((w_gate, 0), (w_value, LANE)):
            src = source.at[:, lanes(s)]
            dst = strip.at[s, block(z, y), pl.ds(at, LANE)]
            if there:
                send(src, dst, w_out.at[s], w_in.at[s], twin).start()
            else:
                pltpu.make_async_copy(src, dst, w_in.at[s]).start()

    def weights_first(first, last):
        def body(s, _):
            pl.when(same)(lambda: weights_away(s, False))
            pl.when(other)(lambda: weights_away(s, True))
            return 0

        lax.fori_loop(first, last, body, 0)

    def upstream_copy(s):
        return send(grad_hidden.at[:, lanes(s)], upstream.at[s], u_out.at[s], u_in.at[s], twin)

    def upstream_first(s, _):
        @pl.when(same)
        def _():
            pltpu.make_async_copy(grad_hidden.at[:, lanes(s)], upstream.at[s], u_in.at[s]).start()

        pl.when(other)(lambda: upstream_copy(s).start())
        return 0

    def token_copies(source, into, out_sem, in_sem):
        copies = []
        for yy in range(2):
            for dx in range(half):
                xx = lax.rem(x + dx, half)
                to = {"fs": z * 2 + yy, "tp": xx * 2 + y}
                dst = into.at[pl.ds(pl.multiple_of(tp * piece, piece), piece)]
                mine = jnp.logical_and(same, yy == y) if dx == 0 else None
                copies.append((mine, source, dst, out_sem.at[yy * half + dx], in_sem.at[tp], to))
        return copies

    def tokens_start(copies):
        for mine, src, dst, out_sem, in_sem, to in copies:
            if mine is None:
                send(src, dst, out_sem, in_sem, to).start()
            else:
                pl.when(mine)(lambda: pltpu.make_async_copy(src, dst, in_sem).start())
                pl.when(jnp.logical_not(mine))(lambda: send(src, dst, out_sem, in_sem, to).start())

    def tokens_sent(copies):
        for mine, src, dst, out_sem, in_sem, to in copies:
            if mine is None:
                send(src, dst, out_sem, in_sem, to).wait_send()
            else:
                pl.when(jnp.logical_not(mine))(lambda: send(src, dst, out_sem, in_sem, to).wait_send())

    def tokens_here(into, in_sem):
        for t in range(tp_n):
            landed(into.at[pl.ds(t * piece, piece)], in_sem.at[t])

    early_copies = token_copies(x_early, early_rows, early_out, early_in)
    late_copies = token_copies(x_late, late_rows, late_out, late_in)
    first = min(3, strips)
    weights_first(0, first)
    conv_copy = send(conv, conv_got, c_out, c_in, partner)
    conv_copy.start()
    tokens_start(early_copies)
    weights_first(first, strips)
    lax.fori_loop(0, strips, upstream_first, 0)
    tokens_start(late_copies)

    def up(s, k):
        at = own_slot(s, z - k, c)
        return send(at, at, up_out.at[s, k], up_in.at[s, k], above)

    def down(s, k):
        at = own_slot(s, z + k, c)
        return send(at, at, down_out.at[s, k], down_in.at[s, k], below)

    def share(s, zz):
        at = own_slot(s, zz, c)
        return send(at, at, share_out.at[s, zz], share_in.at[s, zz], partner)

    def spread(s):
        landed(own_slot(s, z, c), w_in.at[s])
        pl.when(has_up)(lambda: up(s, 0).start())
        pl.when(has_down)(lambda: down(s, 0).start())
        share(s, z).start()

    def hop(s, k):
        @pl.when(z - 1 - k >= 0)
        def _():
            landed(own_slot(s, z - 1 - k, c), up_in.at[s, k])
            pl.when(has_up)(lambda: up(s, k + 1).start())
            share(s, z - 1 - k).start()

        @pl.when(z + 1 + k < depth)
        def _():
            landed(own_slot(s, z + 1 + k, c), down_in.at[s, k])
            pl.when(has_down)(lambda: down(s, k + 1).start())
            share(s, z + 1 + k).start()

    def gathered(s):
        def body(zz, _):
            landed(own_slot(s, zz, 1 - c), share_in.at[s, zz])
            return 0

        lax.fori_loop(0, depth, body, 0)

    def taps_of(s):
        got = jnp.where(same, conv[:, lanes(s)], conv_got[:, lanes(s)])
        return [got[j : j + 1] for j in range(taps_count)]

    def mix(gate, taps):
        position = lax.broadcasted_iota(jnp.int32, gate.shape, 0)
        moved = []
        for j in range(taps_count):
            delay = taps_count - 1 - j
            if delay == 0:
                moved.append(gate)
            else:
                moved.append(jnp.where(position >= delay, pltpu.roll(gate, delay, 0), 0.0))
        pre = moved[0] * taps[0]
        for j in range(1, taps_count):
            pre = pre + moved[j] * taps[j]
        return pre, moved

    def project(source, s):
        both = jnp.dot(source[...], strip[s], preferred_element_type=jnp.float32)
        both = both.astype(jnp.bfloat16).astype(jnp.float32)
        return both[:, :LANE], both[:, LANE:]

    def backward(s):
        landed(upstream.at[s], u_in.at[s])
        gate, value = project(early_rows, s)
        taps = taps_of(s)
        pre, moved = mix(gate, taps)
        cdf = 0.5 * (1.0 + lax.erf(pre * root_half))
        bend = cdf + pre * jnp.exp(-0.5 * pre * pre) * density_norm
        grad = upstream[s].astype(jnp.float32)
        cots[s, :, LANE:] = (grad * (pre * cdf)).astype(cots.dtype)
        slope = grad * value * bend
        for j in range(taps_count):
            taps_own[pl.ds(j, 1), lanes(s)] = jnp.sum(slope * moved[j], axis=0, keepdims=True)
        position = lax.broadcasted_iota(jnp.int32, slope.shape, 0)
        d_gate = slope * taps[taps_count - 1]
        for j in range(taps_count - 1):
            ahead = taps_count - 1 - j
            later = jnp.where(position < tokens - ahead, pltpu.roll(slope, tokens - ahead, 0), 0.0)
            d_gate = d_gate + later * taps[j]
        cots[s, :, :LANE] = d_gate.astype(cots.dtype)

    def term(s, zz, cc):
        return factor * jnp.dot(
            flipped[block(zz, cc), :], cots[s], preferred_element_type=jnp.float32
        )

    def to_partner(s):
        slot = lax.rem(s, 2)
        return send(wire.at[slot], part_got.at[s], q_out.at[slot], q_in.at[s], partner)

    def terms_away(s):
        slot = lax.rem(s, 2)
        pl.when(s >= 2)(lambda: to_partner(s - 2).wait_send())

        def body(zz, _):
            wire[slot, zz] = term(s, zz, 1 - c).astype(wire.dtype)
            return 0

        lax.fori_loop(0, depth, body, 0)
        to_partner(s).start()

    def terms_here(s):
        landed(part_got.at[s], q_in.at[s])

        def body(zz, _):
            value = term(s, zz, c) + part_got[s, zz].astype(jnp.float32)
            part_got[s, zz] = value.astype(part_got.dtype)
            return 0

        lax.fori_loop(0, depth, body, 0)

    def hidden_copy(s, there):
        slot = lax.rem(s, 2)
        src, dst = out_stage.at[slot], hidden.at[:, lanes(s)]
        if there:
            return send(src, dst, h_out.at[slot], h_in.at[s], twin)
        return pltpu.make_async_copy(src, dst, h_out.at[slot])

    def hidden_sent(s):
        pl.when(other)(lambda: hidden_copy(s, True).wait_send())
        pl.when(same)(lambda: hidden_copy(s, False).wait())

    def forward(s):
        slot = lax.rem(s, 2)
        pl.when(s >= 2)(lambda: hidden_sent(s - 2))
        gate, value = project(late_rows, s)
        pre, _ = mix(gate, taps_of(s))
        active = 0.5 * pre * (1.0 + lax.erf(pre * root_half))
        out_stage[slot] = (active * value).astype(out_stage.dtype)
        pl.when(other)(lambda: hidden_copy(s, True).start())
        pl.when(same)(lambda: hidden_copy(s, False).start())

    def along(s, zz, away, upward):
        got, sem, to = (up_got, zup_in, above) if upward else (down_got, zdown_in, below)
        return send(part_got.at[s, zz], got.at[s, away - 1], z_out.at[s, zz], sem.at[s, away - 1], to)

    def pass_on(s, away, upward):
        zz = z + away if upward else z - away
        got, sem = (up_got, zup_in) if upward else (down_got, zdown_in)

        @pl.when(zz < depth if upward else zz >= 0)
        def _():
            if away < depth - 1:

                @pl.when(has_down if upward else has_up)
                def _():
                    landed(got.at[s, away], sem.at[s, away])
                    value = part_got[s, zz].astype(jnp.float32) + got[s, away].astype(jnp.float32)
                    part_got[s, zz] = value.astype(part_got.dtype)

            along(s, zz, away, upward).start()

    def fin(s):
        return send(part_got.at[s, z], fin_got.at[s], f_out.at[s], f_in.at[s], twin)

    def put_total(s, value):
        gate_total[:, lanes(s)] = value[:, :LANE]
        value_total[:, lanes(s)] = value[:, LANE:]

    def finish(s):
        pl.when(has_down)(lambda: landed(up_got.at[s, 0], zup_in.at[s, 0]))
        pl.when(has_up)(lambda: landed(down_got.at[s, 0], zdown_in.at[s, 0]))

        def settle(value):
            pl.when(same)(lambda: put_total(s, value))

            @pl.when(other)
            def _():
                part_got[s, z] = value.astype(part_got.dtype)

        def total(refs_):
            value = part_got[s, z].astype(jnp.float32)
            for ref in refs_:
                value = value + ref[s, 0].astype(jnp.float32)
            settle(value)

        pl.when(jnp.logical_not(has_down))(lambda: total([down_got]))
        pl.when(jnp.logical_not(has_up))(lambda: total([up_got]))
        pl.when(jnp.logical_and(has_up, has_down))(lambda: total([up_got, down_got]))
        pl.when(other)(lambda: fin(s).start())

    def accept(s):
        @pl.when(other)
        def _():
            landed(fin_got.at[s], f_in.at[s])
            put_total(s, fin_got[s].astype(jnp.float32))

    def input_grad():
        contract = (((1,), (1,)), ((), ()))
        wide = 2 * LANE

        def body(b, _):
            at = pl.ds(pl.multiple_of(b * wide, wide), wide)
            total = jnp.zeros((tokens, wide), jnp.float32)
            for s in range(strips):
                total = total + lax.dot_general(
                    cots[s], strip[s, at, :], contract, preferred_element_type=jnp.float32
                )
            partial[:, at] = total.astype(partial.dtype)
            return 0

        lax.fori_loop(0, width // wide, body, 0)

    def partial_rows(t):
        return partial.at[pl.ds(pl.multiple_of(t * piece, piece), piece)]

    def partial_copies(fn_there, fn_here):
        for i in range(1, tp_n + 1):
            t = lax.rem(tp + i, tp_n)
            copy = send(
                partial_rows(t), partial_got.at[role_tp], p_out.at[t], p_in.at[role_tp],
                {"fs": role_fs, "tp": t},
            )
            here = jnp.logical_and(same, t == tp)
            pl.when(jnp.logical_not(here))(lambda: fn_there(copy))
            if fn_here is not None:
                pl.when(here)(
                    lambda: fn_here(
                        pltpu.make_async_copy(partial_rows(t), partial_got.at[role_tp], p_in.at[role_tp])
                    )
                )

    def taps_copies(fn_there, fn_here):
        def body(f, _):
            copy = send(
                taps_own, taps_got.at[role_fs], t_out.at[f], t_in.at[role_fs],
                {"fs": f, "tp": role_tp},
            )
            here = jnp.logical_and(same, f == me)
            pl.when(jnp.logical_not(here))(lambda: fn_there(copy))
            if fn_here is not None:
                pl.when(here)(
                    lambda: fn_here(pltpu.make_async_copy(taps_own, taps_got.at[role_fs], t_in.at[role_fs]))
                )
            return 0

        lax.fori_loop(0, n, body, 0)

    def guarded(s, work):
        pl.when(jnp.logical_and(s >= 0, s < strips))(lambda: work(s))

    def prepare():
        tokens_here(early_rows, early_in)
        conv_copy.wait_recv()
        taps_own[...] = jnp.zeros(taps_own.shape, jnp.float32)
        wide = 2 * LANE
        for b in range(width // wide):
            flipped[b * wide : (b + 1) * wide, :] = early_rows[:, b * wide : (b + 1) * wide].T

    def strip_work(s):
        pl.when(s == 0)(prepare)
        gathered(s)
        backward(s)
        terms_away(s)
        pl.when(s == 0)(lambda: tokens_here(late_rows, late_in))
        forward(s)
        terms_here(s)
        for upward in (True, False):
            pass_on(s, depth - 1, upward)

    def step(t, _):
        guarded(t, spread)
        for k in range(depth - 1):
            guarded(t - 1 - k, lambda s, k=k: hop(s, k))
        guarded(t - lag, strip_work)

        @pl.when(t == strips + lag - 1)
        def _():
            taps_copies(lambda copy: copy.start(), lambda copy: copy.start())
            input_grad()
            partial_copies(lambda copy: copy.start(), lambda copy: copy.start())

        for away in range(depth - 2, 0, -1):
            for upward in (True, False):
                guarded(t - lag - (depth - 1 - away), lambda s: pass_on(s, away, upward))
        guarded(t - lag - (depth - 1), finish)
        guarded(t - lag - depth, accept)
        return 0

    lax.fori_loop(0, strips + lag + depth, step, 0)

    def taps_arrive(f, _):
        landed(taps_got.at[f], t_in.at[f])
        return 0

    lax.fori_loop(0, n, taps_arrive, 0)
    sum_of = taps_got[0]
    for i in range(1, n):
        sum_of = sum_of + taps_got[i]
    taps_total[...] = factor * sum_of

    for t in range(tp_n):
        landed(partial_got.at[t], p_in.at[t])
    total = partial_got[0].astype(jnp.float32)
    for t in range(1, tp_n):
        total = total + partial_got[t].astype(jnp.float32)
    grad_early[...] = total.astype(grad_early.dtype)

    conv_copy.wait_send()
    tokens_sent(early_copies)
    tokens_sent(late_copies)
    taps_copies(lambda copy: copy.wait_send(), None)
    partial_copies(lambda copy: copy.wait_send(), None)
    for s in range(max(0, strips - 2), strips):
        to_partner(s).wait_send()
        hidden_sent(s)

    def drain(s, _):
        @pl.when(other)
        def _():
            landed(own_slot(s, z, c), w_out.at[s])
            upstream_copy(s).wait_send()
            hidden_copy(s, True).wait_recv()
            fin(s).wait_send()

        for k in range(depth - 1):
            pl.when(jnp.logical_and(has_up, z - k >= 0))(lambda k=k: up(s, k).wait_send())
            pl.when(jnp.logical_and(has_down, z + k < depth))(lambda k=k: down(s, k).wait_send())
            away = k + 1
            pl.when(z + away < depth)(lambda away=away: along(s, z + away, away, True).wait_send())
            pl.when(z - away >= 0)(lambda away=away: along(s, z - away, away, False).wait_send())
        lax.fori_loop(0, depth, lambda zz, _: (share(s, zz).wait_send(), 0)[1], 0)
        return 0

    lax.fori_loop(0, strips, drain, 0)


def shards(x_late, x_early, w_gate, w_value, conv_taps, grad_hidden, sum_gate, sum_value, sum_taps):
    n, tp_n = lax.axis_size("fs"), lax.axis_size("tp")
    piece, width = x_early.shape
    rows, columns = w_gate.shape
    tokens = piece * tp_n
    strips, depth = columns // LANE, n // 2
    factor = 1.0 / math.sqrt(tokens * n)
    bf16, f32 = x_early.dtype, jnp.float32
    sems = pltpu.SemaphoreType.DMA
    vmem = pl.BlockSpec(memory_space=pltpu.VMEM)
    hbm = pl.BlockSpec(memory_space=pl.ANY)
    taps_shape = (8, columns)
    hops = depth - 1
    hidden, grad_early, gate_total, value_total, taps_total = pl.pallas_call(
        functools.partial(kernel, n, tp_n, factor),
        out_shape=(
            jax.ShapeDtypeStruct((tokens, columns), bf16),
            jax.ShapeDtypeStruct((piece, width), bf16),
            jax.ShapeDtypeStruct((rows, columns), f32),
            jax.ShapeDtypeStruct((rows, columns), f32),
            jax.ShapeDtypeStruct(taps_shape, f32),
        ),
        in_specs=[hbm] * 4 + [vmem] + [hbm],
        out_specs=(hbm,) + (vmem,) * 4,
        scratch_shapes=[
            pltpu.VMEM((strips, n * rows, 2 * LANE), bf16),
            pltpu.VMEM((tokens, width), bf16),
            pltpu.VMEM((tokens, width), bf16),
            pltpu.VMEM((width, tokens), bf16),
            pltpu.VMEM((strips, tokens, 2 * LANE), bf16),
            pltpu.VMEM((strips, tokens, LANE), bf16),
            pltpu.VMEM((2, tokens, LANE), bf16),
            pltpu.VMEM((2, depth, rows, 2 * LANE), bf16),
            pltpu.VMEM((strips, depth, rows, 2 * LANE), bf16),
            pltpu.VMEM((strips, hops, rows, 2 * LANE), bf16),
            pltpu.VMEM((strips, hops, rows, 2 * LANE), bf16),
            pltpu.VMEM((strips, rows, 2 * LANE), bf16),
            pltpu.VMEM((tokens, width), bf16),
            pltpu.VMEM((tp_n, piece, width), bf16),
            pltpu.VMEM(taps_shape, f32),
            pltpu.VMEM((n,) + taps_shape, f32),
            pltpu.VMEM(conv_taps.shape, f32),
        ]
        + [sems((strips,))] * 2
        + [sems((strips, hops))] * 4
        + [sems((strips, depth))] * 2
        + [sems((strips,))] * 2
        + [sems((2,)), sems((strips,))]
        + [sems((2,)), sems((strips,))]
        + [sems((strips, depth)), sems((strips, hops)), sems((strips, hops))]
        + [sems((strips,))] * 2
        + [sems((tp_n,))] * 6
        + [sems((n,))] * 2
        + [sems, sems],
        compiler_params=pltpu.CompilerParams(
            collective_id=0, has_side_effects=True, vmem_limit_bytes=67043328
        ),
        name="layer",
    )(x_late, x_early, w_gate, w_value, conv_taps, grad_hidden)
    return (
        hidden,
        grad_early,
        sum_gate + gate_total,
        sum_value + value_total,
        sum_taps + taps_total[: conv_taps.shape[0]],
    )


def solution(mesh):
    placed = (
        P(("fs", "tp"), None),
        P(("fs", "tp"), None),
        P("fs", "tp"),
        P("fs", "tp"),
        P(None, "tp"),
        P("fs", "tp"),
        P("fs", "tp"),
        P("fs", "tp"),
        P(None, "tp"),
    )
    return jax.shard_map(
        shards,
        mesh=mesh,
        in_specs=placed,
        out_specs=(
            P("fs", "tp"),
            P(("fs", "tp"), None),
            P("fs", "tp"),
            P("fs", "tp"),
            P(None, "tp"),
        ),
        check_vma=False,
    )
```

time: 324 us -> 275 us (0.85); the launches traced: 320 us -> 275 us
  matrix products: 26.3 us -> 0 us
  between operations: 14 us -> 0.65 us
  other arithmetic: 19.1 us -> 5.86 us
  Pallas kernels: 252 us -> 265 us
  local copies, waits for them, and re-layouts: 6.95 us -> 3.44 us
    dot_general x4 -> x0, matrix products: 26.3 us -> none  [the longest x1 8.55 us: shards(): jnp.dot(gathered, gate_full, preferred_element_type=jnp.float32)]
    pallas_call x2 -> x1, Pallas kernels: 252 us -> 265 us  [shards(): pl.pallas_call(functools.partial(kernel, n, tp_n, factor), out_shape=(jax...]
    convert_element_type x1 -> x0, other arithmetic: 10.9 us -> none  [shards(): (upstream * jax.nn.gelu(mixed_pre, approximate=False)).astype(jnp.bfloat16)]
  transfers between devices with their start and end apart: 3 -> 0, of which waited for: 0 -> 0; matrix products, arithmetic and copies ran while one was open for 16% -> 0% of each run, Pallas kernels for 79% -> 0%
where the time goes in v1:
time: 275 us
  Pallas kernels  265 us (96%)
  other arithmetic  5.86 us (2%)
  local copies, waits for them, and re-layouts  3.44 us (1%)
    pallas_call x1, Pallas kernels, shards(): pl.pallas_call(functools.partial(kernel, n, tp_n, factor), out_shape=(jax...  265 us

profile of v1, /device:TPU:1, one launch (start us, length us, event | category | flops | bytes accessed | tf_op | source)
XLA Modules:
  0.0 275.0 jit_solution(6362425615218669102)
XLA Ops:
  0.6 265.0 %layer.1 = (bf16[768,1408]{1,0:T(8,128)(2,1)}, bf16[192,2048]{1,0:T(8,128)(2,1)}, f32[256,1408]{1,0:T(8,128)}, f32[256,1408]{1,0:T(8,128)}, f32[8,1408]{1,0:T(8,128)}) custom-call(bf16[192,2048]{1,0:T(8,128)(2,1)} %refs_0_.1, bf16[192,2048]{1,0:T(8,128)(2,1)} %refs_1_.1, bf16[256,1408]{1,0:T(8,128)(2,1)} %refs_2_.1, bf16[256,1408]{1,0:T(8,128)(2,1)} %refs_3_.1, ...), custom_call_target="tpu_custom_call" | custom-call | tf_op jit(solution)/shard_map/layer/pallas_call | solution.py:497
  265.7 1.4 slice_add_fusion
  267.1 0.0 copy-start.1
  267.1 0.0 copy-start.2
  267.1 3.2 %add.9 = f32[256,1408]{1,0:T(8,128)} add(f32[256,1408]{1,0:T(8,128)} %param.15, f32[256,1408]{1,0:T(8,128)} %get-tuple-element.12) | non-fusion elementwise | flops 360448 | bytes 4325376 | tf_op jit(solution)/shard_map/add | solution.py:546
  270.3 0.0 copy-done.1
  270.3 0.0 copy-done.2
  270.3 0.0 copy-start
  270.3 1.2 add.10
  271.5 0.9 copy-done
  272.4 0.0 copy-start.3
  272.4 1.3 copy.16
  273.8 0.3 copy-done.3
  274.1 0.9 copy.17
Async XLA Ops:
  267.1 3.2 %copy-start.1 = (f32[256,1408]{1,0:T(8,128)S(1)}, f32[256,1408]{1,0:T(8,128)}, u32[]{:S(2)}) copy-start(f32[256,1408]{1,0:T(8,128)} %param.16) | copy-start | bytes 4325380
  267.1 3.2 %copy-start.2 = (f32[256,1408]{1,0:T(8,128)S(1)}, f32[256,1408]{1,0:T(8,128)}, u32[]{:S(2)}) copy-start(f32[256,1408]{1,0:T(8,128)} %get-tuple-element.13) | copy-start | bytes 4325380
  270.3 2.1 copy-start
  272.4 1.7 copy-start.3

commit v2 on v1

--- a/solution.py
+++ b/solution.py
@@ -12,29 +12,42 @@
 density_norm = 0.3989422804014327
 MESH = pl.DeviceIdType.MESH
 LANE = 128
-LEAD = 2
+HOP = 2
+BEHIND = 5
+DELAY = 1
+FLUSH = 1
+PER_STEP = 2
+GROUPS = (7, 3)
+TURN = 2
 
 
 def kernel(n, tp_n, factor, *refs):
-    x_late, x_early, w_gate, w_value, conv, grad_hidden = refs[:6]
-    hidden, grad_early, gate_total, value_total, taps_total = refs[6:11]
+    x_late, x_early, w_gate, w_value, conv, grad_hidden, sum_gate, sum_value, sum_taps = refs[:9]
+    hidden, grad_early, new_gate, new_value, new_taps = refs[9:14]
     (
         strip, late_rows, early_rows, flipped, cots, upstream, out_stage, wire, part_got,
-        up_got, down_got, fin_got, partial, partial_got, taps_own, taps_got, conv_got,
-    ) = refs[11:28]
+        up_got, down_got, fin_got, partial, partial_got, taps_own, taps_got, conv_got, ahead,
+        gate_total, value_total,
+    ) = refs[14:34]
     (
         w_out, w_in, up_out, up_in, down_out, down_in, share_out, share_in, u_out, u_in,
         h_out, h_in, q_out, q_in, z_out, zup_in, zdown_in, f_out, f_in, late_out, late_in,
-        early_out, early_in, p_out, p_in, t_out, t_in, c_out, c_in,
-    ) = refs[28:]
+        early_out, early_in, late_pass, early_pass, p_out, p_in, t_out, t_in, c_out, c_in,
+        sums_in, sums_out,
+    ) = refs[34:]
     depth, half = n // 2, tp_n // 2
-    rows = gate_total.shape[0]
-    columns = gate_total.shape[1]
+    rows, columns = gate_total.shape
     strips = columns // LANE
     tokens, width = early_rows.shape
     piece = x_early.shape[0]
     taps_count = conv.shape[0]
-    lag = depth + LEAD
+    lag = HOP + depth - 1
+    late_at = lag + BEHIND
+    last_hop = lag + depth - 2
+    flush = max(strips + lag - FLUSH, last_hop)
+    parts = early_in.shape[1]
+    part = piece // parts
+    groups = [0] + [strips - k for k in GROUPS if strips > k] + [strips]
     me, tp = lax.axis_index("fs"), lax.axis_index("tp")
     z, y = lax.div(me, 2), lax.rem(me, 2)
     x, c = lax.div(tp, 2), lax.rem(tp, 2)
@@ -113,15 +126,16 @@
         pl.when(other)(lambda: upstream_copy(s).start())
         return 0
 
-    def token_copies(source, into, out_sem, in_sem):
+    def token_part(into, t, q):
+        return into.at[pl.ds(pl.multiple_of(t * piece + q * part, part), part)]
+
+    def token_copies(source, into, out_sem, in_sem, q):
         copies = []
-        for yy in range(2):
-            for dx in range(half):
-                xx = lax.rem(x + dx, half)
-                to = {"fs": z * 2 + yy, "tp": xx * 2 + y}
-                dst = into.at[pl.ds(pl.multiple_of(tp * piece, piece), piece)]
-                mine = jnp.logical_and(same, yy == y) if dx == 0 else None
-                copies.append((mine, source, dst, out_sem.at[yy * half + dx], in_sem.at[tp], to))
+        for i, (dx, yy) in enumerate([(0, 1 - y)] + [(dx, y) for dx in range(1, half)] + [(0, y)]):
+            to = {"fs": z * 2 + yy, "tp": lax.rem(x + dx, half) * 2 + y}
+            mine = same if i == half else None
+            src = source.at[pl.ds(q * part, part)]
+            copies.append((mine, src, token_part(into, tp, q), out_sem.at[i, q], in_sem.at[tp, q], to))
         return copies
 
     def tokens_start(copies):
@@ -139,20 +153,63 @@
             else:
                 pl.when(jnp.logical_not(mine))(lambda: send(src, dst, out_sem, in_sem, to).wait_send())
 
+    def turn(into, in_sem, pass_sem, cc, dx, q):
+        t = x * 2 + cc
+        at = token_part(into, t, q)
+        to = {"fs": me, "tp": lax.rem(x + dx, half) * 2 + c}
+        return send(at, at, pass_sem.at[cc * half + dx, q], in_sem.at[t, q], to)
+
+    def tokens_turn(into, in_sem, pass_sem, q):
+        @pl.when(other)
+        def _():
+            for cc in range(2):
+                landed(token_part(into, x * 2 + cc, q), in_sem.at[x * 2 + cc, q])
+                for dx in range(1, half):
+                    turn(into, in_sem, pass_sem, cc, dx, q).start()
+
+    def turned(into, in_sem, pass_sem):
+        @pl.when(other)
+        def _():
+            for q in range(parts):
+                for dx in range(1, half):
+                    for cc in range(2):
+                        turn(into, in_sem, pass_sem, cc, dx, q).wait_send()
+
     def tokens_here(into, in_sem):
         for t in range(tp_n):
-            landed(into.at[pl.ds(t * piece, piece)], in_sem.at[t])
-
-    early_copies = token_copies(x_early, early_rows, early_out, early_in)
-    late_copies = token_copies(x_late, late_rows, late_out, late_in)
-    first = min(3, strips)
+
+            @pl.when(jnp.logical_or(same, x != t // 2))
+            def _():
+                for q in range(parts):
+                    landed(token_part(into, t, q), in_sem.at[t, q])
+
+    early_copies = [token_copies(x_early, early_rows, early_out, early_in, q) for q in range(parts)]
+    late_copies = [token_copies(x_late, late_rows, late_out, late_in, q) for q in range(parts)]
+    first = min(2, strips)
     weights_first(0, first)
     conv_copy = send(conv, conv_got, c_out, c_in, partner)
     conv_copy.start()
-    tokens_start(early_copies)
-    weights_first(first, strips)
-    lax.fori_loop(0, strips, upstream_first, 0)
-    tokens_start(late_copies)
+    for q in range(parts):
+        tokens_start(early_copies[q])
+        weights_first(min(first + q, strips), min(first + q + 1, strips))
+    soon = min(first + parts, strips)
+    head = min(4, strips)
+
+    def second_wave():
+        def body(s, _):
+            pl.when(s < head)(lambda: (upstream_first(s, 0), None)[1])
+            at = soon + 2 * s
+            for i in range(2):
+                pl.when(at + i < strips)(lambda: weights_first(at + i, at + i + 1))
+            return 0
+
+        lax.fori_loop(0, max(head, -(-(strips - soon) // 2)), body, 0)
+
+    def third_wave():
+        for q in range(parts):
+            tokens_start(late_copies[q])
+            lax.fori_loop(min(head + q, strips), min(head + q + 1, strips), upstream_first, 0)
+        lax.fori_loop(min(head + parts, strips), strips, upstream_first, 0)
 
     def up(s, k):
         at = own_slot(s, z - k, c)
@@ -292,9 +349,10 @@
 
     def pass_on(s, away, upward):
         zz = z + away if upward else z - away
+        inside = zz < depth if upward else zz >= 0
         got, sem = (up_got, zup_in) if upward else (down_got, zdown_in)
 
-        @pl.when(zz < depth if upward else zz >= 0)
+        @pl.when(inside)
         def _():
             if away < depth - 1:
 
@@ -309,9 +367,20 @@
     def fin(s):
         return send(part_got.at[s, z], fin_got.at[s], f_out.at[s], f_in.at[s], twin)
 
+    sums = ((sum_gate, gate_total, new_gate), (sum_value, value_total, new_value))
+
+    def sum_load(i):
+        return pltpu.make_async_copy(sums[i][0], sums[i][1], sums_in.at[i])
+
+    def sum_store(i, s):
+        at = (slice(None), lanes(s))
+        return pltpu.make_async_copy(sums[i][1].at[at], sums[i][2].at[at], sums_out.at[s, i])
+
     def put_total(s, value):
-        gate_total[:, lanes(s)] = value[:, :LANE]
-        value_total[:, lanes(s)] = value[:, LANE:]
+        gate_total[:, lanes(s)] += value[:, :LANE]
+        value_total[:, lanes(s)] += value[:, LANE:]
+        for i in range(2):
+            sum_store(i, s).start()
 
     def finish(s):
         pl.when(has_down)(lambda: landed(up_got.at[s, 0], zup_in.at[s, 0]))
@@ -341,40 +410,63 @@
             landed(fin_got.at[s], f_in.at[s])
             put_total(s, fin_got[s].astype(jnp.float32))
 
+    wide = 2 * LANE
+    blocks = width // wide
+
+    def grad_block(b, first, last):
+        at = pl.ds(pl.multiple_of(b * wide, wide), wide)
+        total = jnp.zeros((tokens, wide), jnp.float32)
+        for s in range(first, last):
+            total = total + lax.dot_general(
+                cots[s], strip[s, at, :], (((1,), (1,)), ((), ())), preferred_element_type=jnp.float32
+            )
+        return at, total
+
+    def input_grad_ahead(s):
+        for g in range(len(groups) - 2):
+            start, end = groups[g + 1], groups[g + 2]
+            share_of = -(-blocks // (end - start))
+
+            @pl.when(jnp.logical_and(s >= start, s < end))
+            def _():
+                first = (s - start) * share_of
+
+                def body(b, _):
+                    at, total = grad_block(b, groups[g], start)
+                    if g > 0:
+                        total = total + ahead[:, at]
+                    ahead[:, at] = total
+                    return 0
+
+                lax.fori_loop(jnp.minimum(first, blocks), jnp.minimum(first + share_of, blocks), body, 0)
+
     def input_grad():
-        contract = (((1,), (1,)), ((), ()))
-        wide = 2 * LANE
-
         def body(b, _):
-            at = pl.ds(pl.multiple_of(b * wide, wide), wide)
-            total = jnp.zeros((tokens, wide), jnp.float32)
-            for s in range(strips):
-                total = total + lax.dot_general(
-                    cots[s], strip[s, at, :], contract, preferred_element_type=jnp.float32
-                )
+            at, total = grad_block(b, groups[-2], strips)
+            if len(groups) > 2:
+                total = total + ahead[:, at]
             partial[:, at] = total.astype(partial.dtype)
             return 0
 
-        lax.fori_loop(0, width // wide, body, 0)
+        lax.fori_loop(0, blocks, body, 0)
 
     def partial_rows(t):
         return partial.at[pl.ds(pl.multiple_of(t * piece, piece), piece)]
 
-    def partial_copies(fn_there, fn_here):
-        for i in range(1, tp_n + 1):
-            t = lax.rem(tp + i, tp_n)
-            copy = send(
-                partial_rows(t), partial_got.at[role_tp], p_out.at[t], p_in.at[role_tp],
-                {"fs": role_fs, "tp": t},
+    def partial_copy(i, fn_there, fn_here):
+        t = lax.rem(tp + i, tp_n)
+        copy = send(
+            partial_rows(t), partial_got.at[role_tp], p_out.at[t], p_in.at[role_tp],
+            {"fs": role_fs, "tp": t},
+        )
+        here = jnp.logical_and(same, t == tp)
+        pl.when(jnp.logical_not(here))(lambda: fn_there(copy))
+        if fn_here is not None:
+            pl.when(here)(
+                lambda: fn_here(
+                    pltpu.make_async_copy(partial_rows(t), partial_got.at[role_tp], p_in.at[role_tp])
+                )
             )
-            here = jnp.logical_and(same, t == tp)
-            pl.when(jnp.logical_not(here))(lambda: fn_there(copy))
-            if fn_here is not None:
-                pl.when(here)(
-                    lambda: fn_here(
-                        pltpu.make_async_copy(partial_rows(t), partial_got.at[role_tp], p_in.at[role_tp])
-                    )
-                )
 
     def taps_copies(fn_there, fn_here):
         def body(f, _):
@@ -392,10 +484,15 @@
 
         lax.fori_loop(0, n, body, 0)
 
+    for i in range(2):
+        sum_load(i).start()
+
     def guarded(s, work):
-        pl.when(jnp.logical_and(s >= 0, s < strips))(lambda: work(s))
+        pl.when(jnp.logical_and(s >= 0, s < strips))(lambda: (work(s), None)[1])
 
     def prepare():
+        for i in range(2):
+            sum_load(i).wait()
         tokens_here(early_rows, early_in)
         conv_copy.wait_recv()
         taps_own[...] = jnp.zeros(taps_own.shape, jnp.float32)
@@ -403,37 +500,76 @@
         for b in range(width // wide):
             flipped[b * wide : (b + 1) * wide, :] = early_rows[:, b * wide : (b + 1) * wide].T
 
+    def delayed(t, at, steps, work):
+        until = flush + at - last_hop
+        pl.when(t < until)(lambda: guarded(t - at - steps, work))
+
+        @pl.when(t == until)
+        def _():
+            lax.fori_loop(
+                jnp.maximum(0, until - at - steps), min(strips, until - at),
+                lambda s, _: (work(s), 0)[1], 0,
+            )
+
+        pl.when(t >= until)(lambda: guarded(t - at, work))
+
     def strip_work(s):
         pl.when(s == 0)(prepare)
         gathered(s)
         backward(s)
         terms_away(s)
+
+    def late_work(s):
         pl.when(s == 0)(lambda: tokens_here(late_rows, late_in))
         forward(s)
+
+    def own_work(s):
         terms_here(s)
         for upward in (True, False):
             pass_on(s, depth - 1, upward)
+        input_grad_ahead(s)
 
     def step(t, _):
         guarded(t, spread)
         for k in range(depth - 1):
-            guarded(t - 1 - k, lambda s, k=k: hop(s, k))
+            guarded(t - HOP - k, lambda s, k=k: hop(s, k))
+
+        for q in range(parts):
+            pl.when(t == min(1 + (q + 1) // 2, lag - 1))(
+                lambda: tokens_turn(early_rows, early_in, early_pass, q)
+            )
+            pl.when(t == min(lag + TURN + q, late_at - 1))(
+                lambda: tokens_turn(late_rows, late_in, late_pass, q)
+            )
+        pl.when(t == min(3, lag - 1))(second_wave)
         guarded(t - lag, strip_work)
+
+        for j in range(2):
+            guarded(2 * (t - late_at) + j, late_work)
+        guarded(t - lag, own_work)
+        pl.when(t == lag)(third_wave)
 
         @pl.when(t == strips + lag - 1)
         def _():
             taps_copies(lambda copy: copy.start(), lambda copy: copy.start())
             input_grad()
-            partial_copies(lambda copy: copy.start(), lambda copy: copy.start())
 
         for away in range(depth - 2, 0, -1):
             for upward in (True, False):
-                guarded(t - lag - (depth - 1 - away), lambda s: pass_on(s, away, upward))
-        guarded(t - lag - (depth - 1), finish)
-        guarded(t - lag - depth, accept)
+                links = z if upward else depth - 1 - z
+                delayed(
+                    t, lag + depth - 1 - away, DELAY * links, lambda s: pass_on(s, away, upward)
+                )
+        links = jnp.maximum(jnp.where(has_down, z - 1, 0), jnp.where(has_up, depth - 2 - z, 0))
+        delayed(t, last_hop + 1, DELAY * links, finish)
+        delayed(t, last_hop + 2, DELAY * links, accept)
+        for i in range(tp_n):
+            pl.when(t == strips + lag - 1 + i // PER_STEP)(
+                lambda: partial_copy(tp_n - i, lambda copy: copy.start(), lambda copy: copy.start())
+            )
         return 0
 
-    lax.fori_loop(0, strips + lag + depth, step, 0)
+    lax.fori_loop(0, max(strips + lag + max(depth, tp_n), late_at + strips // 2 + 1), step, 0)
 
     def taps_arrive(f, _):
         landed(taps_got.at[f], t_in.at[f])
@@ -443,7 +579,7 @@
     sum_of = taps_got[0]
     for i in range(1, n):
         sum_of = sum_of + taps_got[i]
-    taps_total[...] = factor * sum_of
+    new_taps[...] = sum_taps[...] + factor * sum_of[:taps_count]
 
     for t in range(tp_n):
         landed(partial_got.at[t], p_in.at[t])
@@ -453,15 +589,22 @@
     grad_early[...] = total.astype(grad_early.dtype)
 
     conv_copy.wait_send()
-    tokens_sent(early_copies)
-    tokens_sent(late_copies)
+    for q in range(parts):
+        tokens_sent(early_copies[q])
+        tokens_sent(late_copies[q])
+    turned(early_rows, early_in, early_pass)
+    turned(late_rows, late_in, late_pass)
     taps_copies(lambda copy: copy.wait_send(), None)
-    partial_copies(lambda copy: copy.wait_send(), None)
+    for i in range(tp_n):
+        partial_copy(i, lambda copy: copy.wait_send(), None)
     for s in range(max(0, strips - 2), strips):
         to_partner(s).wait_send()
         hidden_sent(s)
 
     def drain(s, _):
+        for i in range(2):
+            sum_store(i, s).wait()
+
         @pl.when(other)
         def _():
             landed(own_slot(s, z, c), w_out.at[s])
@@ -494,17 +637,18 @@
     hbm = pl.BlockSpec(memory_space=pl.ANY)
     taps_shape = (8, columns)
     hops = depth - 1
-    hidden, grad_early, gate_total, value_total, taps_total = pl.pallas_call(
+    parts = next(q for q in (4, 2, 1) if piece % (16 * q) == 0)
+    return pl.pallas_call(
         functools.partial(kernel, n, tp_n, factor),
         out_shape=(
             jax.ShapeDtypeStruct((tokens, columns), bf16),
             jax.ShapeDtypeStruct((piece, width), bf16),
             jax.ShapeDtypeStruct((rows, columns), f32),
             jax.ShapeDtypeStruct((rows, columns), f32),
-            jax.ShapeDtypeStruct(taps_shape, f32),
+            jax.ShapeDtypeStruct(sum_taps.shape, f32),
         ),
-        in_specs=[hbm] * 4 + [vmem] + [hbm],
-        out_specs=(hbm,) + (vmem,) * 4,
+        in_specs=[hbm] * 4 + [vmem] + [hbm] * 3 + [vmem],
+        out_specs=(hbm, vmem, hbm, hbm, vmem),
         scratch_shapes=[
             pltpu.VMEM((strips, n * rows, 2 * LANE), bf16),
             pltpu.VMEM((tokens, width), bf16),
@@ -523,6 +667,9 @@
             pltpu.VMEM(taps_shape, f32),
             pltpu.VMEM((n,) + taps_shape, f32),
             pltpu.VMEM(conv_taps.shape, f32),
+            pltpu.VMEM((tokens, width), f32),
+            pltpu.VMEM((rows, columns), f32),
+            pltpu.VMEM((rows, columns), f32),
         ]
         + [sems((strips,))] * 2
         + [sems((strips, hops))] * 4
@@ -532,20 +679,17 @@
         + [sems((2,)), sems((strips,))]
         + [sems((strips, depth)), sems((strips, hops)), sems((strips, hops))]
         + [sems((strips,))] * 2
-        + [sems((tp_n,))] * 6
+        + [sems((tp_n, parts))] * 6
+        + [sems((tp_n,))] * 2
         + [sems((n,))] * 2
-        + [sems, sems],
+        + [sems, sems]
+        + [sems((2,)), sems((strips, 2))],
         compiler_params=pltpu.CompilerParams(
             collective_id=0, has_side_effects=True, vmem_limit_bytes=67043328
         ),
         name="layer",
-    )(x_late, x_early, w_gate, w_value, conv_taps, grad_hidden)
-    return (
-        hidden,
-        grad_early,
-        sum_gate + gate_total,
-        sum_value + value_total,
-        sum_taps + taps_total[: conv_taps.shape[0]],
+    )(
+        x_late, x_early, w_gate, w_value, conv_taps, grad_hidden, sum_gate, sum_value, sum_taps
     )
 
 

time: 275 us -> 202 us (0.73)
  Pallas kernels: 265 us -> 193 us
  other arithmetic: 5.86 us -> 0 us
  local copies, waits for them, and re-layouts: 3.44 us -> 8.42 us
    pallas_call x1, Pallas kernels: 265 us -> 193 us  [shards(): pl.pallas_call(functools.partial(kernel, n, tp_n, factor), out_shape=(jax...]
    add x3 -> x0, other arithmetic: 5.86 us -> none  [the longest x1 3.19 us: shards(): sum_gate + gate_total]
    unnamed x10 -> x13, local copies, waits for them, and re-layouts: 3.44 us -> 8.42 us
where the time goes in v2:
time: 202 us
  Pallas kernels  193 us (96%)
  local copies, waits for them, and re-layouts  8.42 us (4%)
    pallas_call x1, Pallas kernels, shards(): pl.pallas_call(functools.partial(kernel, n, tp_n, factor), out_shape=(jax...  193 us
    unnamed x13, local copies, waits for them, and re-layouts  8.42 us

profile of v2, /device:TPU:1, one launch (start us, length us, event | category | flops | bytes accessed | tf_op | source)
XLA Modules:
  0.0 202.2 jit_solution(18059390234813554577)
XLA Ops:
  0.6 193.1 %layer.1 = (bf16[768,1408]{1,0:T(8,128)(2,1)}, bf16[192,2048]{1,0:T(8,128)(2,1)}, f32[256,1408]{1,0:T(8,128)}, f32[256,1408]{1,0:T(8,128)}, f32[3,1408]{1,0:T(4,128)}) custom-call(bf16[192,2048]{1,0:T(8,128)(2,1)} %refs_0_.1, bf16[192,2048]{1,0:T(8,128)(2,1)} %refs_1_.1, bf16[256,1408]{1,0:T(8,128)(2,1)} %refs_2_.1, bf16[256,1408]{1,0:T(8,128)(2,1)} %refs_3_.1, ...), custom_call_target="tpu_custom_call" | custom-call | tf_op jit(solution)/shard_map/layer/pallas_call | solution.py:641
  193.7 0.0 copy-start.2
  193.7 3.2 %copy.19 = bf16[768,1408]{1,0:T(8,128)(2,1)} copy(bf16[768,1408]{1,0:T(8,128)(2,1)} %get-tuple-element.10) | data formatting | bytes 4325376
  196.9 0.0 copy-done.2
  196.9 0.0 copy-start.1
  196.9 0.9 copy.20
  197.8 0.8 copy-done.1
  198.6 0.0 copy-start
  198.6 1.1 copy.21
  199.7 0.8 copy-done
  200.4 0.0 copy-start.3
  200.5 1.1 copy.22
  201.6 0.0 copy-done.3
  201.6 0.6 copy.23
Async XLA Ops:
  193.7 3.2 %copy-start.2 = (bf16[192,2048]{1,0:T(8,128)(2,1)S(1)}, bf16[192,2048]{1,0:T(8,128)(2,1)}, u32[]{:S(2)}) copy-start(bf16[192,2048]{1,0:T(8,128)(2,1)} %get-tuple-element.11) | copy-start | bytes 2359300
  196.9 1.6 copy-start.1
  198.6 1.9 copy-start
  200.4 1.1 copy-start.3

commit v3 on v2

--- a/solution.py
+++ b/solution.py
@@ -16,7 +16,9 @@
 BEHIND = 5
 DELAY = 1
 FLUSH = 1
-PER_STEP = 2
+LATER = 1
+JOIN = (2, 4)
+MEET = 3
 GROUPS = (7, 3)
 TURN = 2
 
@@ -26,15 +28,16 @@
     hidden, grad_early, new_gate, new_value, new_taps = refs[9:14]
     (
         strip, late_rows, early_rows, flipped, cots, upstream, out_stage, wire, part_got,
-        up_got, down_got, fin_got, partial, partial_got, taps_own, taps_got, conv_got, ahead,
-        gate_total, value_total,
-    ) = refs[14:34]
+        up_got, down_got, fin_got, partial_got, taps_own, taps_got, conv_got, ahead,
+        gate_total, value_total, mid_got, far_got,
+    ) = refs[14:35]
     (
         w_out, w_in, up_out, up_in, down_out, down_in, share_out, share_in, u_out, u_in,
         h_out, h_in, q_out, q_in, z_out, zup_in, zdown_in, f_out, f_in, late_out, late_in,
         early_out, early_in, late_pass, early_pass, p_out, p_in, t_out, t_in, c_out, c_in,
-        sums_in, sums_out,
-    ) = refs[34:]
+        sums_in, sums_out, m_out, m_in, a_out, a_in,
+    ) = refs[35:]
+    partial = late_rows
     depth, half = n // 2, tp_n // 2
     rows, columns = gate_total.shape
     strips = columns // LANE
@@ -42,9 +45,10 @@
     piece = x_early.shape[0]
     taps_count = conv.shape[0]
     lag = HOP + depth - 1
-    late_at = lag + BEHIND
+    late_at = lag + min(BEHIND, strips - 1 - (strips - 1) // 2)
     last_hop = lag + depth - 2
     flush = max(strips + lag - FLUSH, last_hop)
+    ended = strips + lag - 1
     parts = early_in.shape[1]
     part = piece // parts
     groups = [0] + [strips - k for k in GROUPS if strips > k] + [strips]
@@ -292,10 +296,9 @@
             d_gate = d_gate + later * taps[j]
         cots[s, :, :LANE] = d_gate.astype(cots.dtype)
 
-    def term(s, zz, cc):
-        return factor * jnp.dot(
-            flipped[block(zz, cc), :], cots[s], preferred_element_type=jnp.float32
-        )
+    def terms(s, cc):
+        made = factor * jnp.dot(flipped[cc], cots[s], preferred_element_type=jnp.float32)
+        return made.reshape(depth, rows, 2 * LANE)
 
     def to_partner(s):
         slot = lax.rem(s, 2)
@@ -305,22 +308,12 @@
         slot = lax.rem(s, 2)
         pl.when(s >= 2)(lambda: to_partner(s - 2).wait_send())
 
-        def body(zz, _):
-            wire[slot, zz] = term(s, zz, 1 - c).astype(wire.dtype)
-            return 0
-
-        lax.fori_loop(0, depth, body, 0)
+        wire[slot] = terms(s, 1 - c).astype(wire.dtype)
         to_partner(s).start()
 
     def terms_here(s):
         landed(part_got.at[s], q_in.at[s])
-
-        def body(zz, _):
-            value = term(s, zz, c) + part_got[s, zz].astype(jnp.float32)
-            part_got[s, zz] = value.astype(part_got.dtype)
-            return 0
-
-        lax.fori_loop(0, depth, body, 0)
+        part_got[s] = (terms(s, c) + part_got[s].astype(jnp.float32)).astype(part_got.dtype)
 
     def hidden_copy(s, there):
         slot = lax.rem(s, 2)
@@ -453,20 +446,118 @@
     def partial_rows(t):
         return partial.at[pl.ds(pl.multiple_of(t * piece, piece), piece)]
 
-    def partial_copy(i, fn_there, fn_here):
-        t = lax.rem(tp + i, tp_n)
-        copy = send(
-            partial_rows(t), partial_got.at[role_tp], p_out.at[t], p_in.at[role_tp],
-            {"fs": role_fs, "tp": t},
+    def partial_add(t, gots):
+        at = pl.ds(pl.multiple_of(t * piece, piece), piece)
+        total = partial[at, :].astype(jnp.float32)
+        for got in gots:
+            total = total + got[...].astype(jnp.float32)
+        partial[at, :] = total.astype(partial.dtype)
+
+    def direct(dx, cc):
+        t = lax.rem(x + dx, half) * 2 + cc
+        return send(
+            partial_rows(t), partial_got.at[x], p_out.at[t], p_in.at[x], {"fs": me, "tp": t}
         )
-        here = jnp.logical_and(same, t == tp)
-        pl.when(jnp.logical_not(here))(lambda: fn_there(copy))
-        if fn_here is not None:
-            pl.when(here)(
-                lambda: fn_here(
-                    pltpu.make_async_copy(partial_rows(t), partial_got.at[role_tp], p_in.at[role_tp])
-                )
-            )
+
+    def direct_start(dx, cc):
+        if dx > 0:
+            direct(dx, cc).start()
+        else:
+            here = pltpu.make_async_copy(partial_rows(tp), partial_got.at[x], p_in.at[x])
+            pl.when(cc == c)(lambda: here.start())
+            pl.when(cc != c)(lambda: direct(dx, cc).start())
+
+    def across(dx):
+        xx = lax.rem(x + dx, half)
+        return send(
+            partial_rows(xx * 2), mid_got.at[dx - 1], m_out.at[dx - 1], m_in.at[dx - 1],
+            {"fs": me, "tp": xx * 2 + c},
+        )
+
+    def over():
+        return send(
+            partial_rows(x * 2), partial_got.at[half], p_out.at[0], p_in.at[half],
+            {"fs": role_fs, "tp": x * 2},
+        )
+
+    def away_y(dx):
+        t = lax.rem(x + dx, half) * 2 + 1
+        return send(
+            partial_rows(t), far_got.at[dx], a_out.at[dx], a_in.at[dx], {"fs": role_fs, "tp": tp}
+        )
+
+    order = tuple(range(1, half)) + (0,)
+
+    def partial_start():
+        @pl.when(other)
+        def _():
+            for dx in range(1, half):
+                across(dx).start()
+            for dx in order:
+                away_y(dx).start()
+
+        pl.when(same)(lambda: direct_start(0, 0))
+
+    def partial_far():
+        @pl.when(same)
+        def _():
+            for dx in range(1, half):
+                direct_start(dx, 0)
+
+    def partial_joined(dx):
+        @pl.when(same)
+        def _():
+            landed(far_got.at[dx], a_in.at[dx])
+            partial_add(lax.rem(x + dx, half) * 2 + 1, [far_got.at[dx]])
+            direct_start(dx, 1)
+
+    def partial_over():
+        @pl.when(other)
+        def _():
+            for dx in range(1, half):
+                landed(mid_got.at[dx - 1], m_in.at[dx - 1])
+            if half > 1:
+                partial_add(x * 2, [mid_got.at[dx - 1] for dx in range(1, half)])
+            over().start()
+
+    def partial_sent():
+        @pl.when(same)
+        def _():
+            for dx in range(half):
+                for cc in range(2):
+                    if dx > 0:
+                        direct(dx, cc).wait_send()
+                    else:
+                        pl.when(cc != c)(lambda: direct(dx, cc).wait_send())
+
+        @pl.when(other)
+        def _():
+            over().wait_send()
+            for dx in range(half):
+                away_y(dx).wait_send()
+                if dx > 0:
+                    across(dx).wait_send()
+
+    def partial_total():
+        for i in range(half):
+            landed(partial_got.at[i], p_in.at[i])
+        total = partial_got[0].astype(jnp.float32)
+        for i in range(1, half):
+            total = total + partial_got[i].astype(jnp.float32)
+
+        @pl.when(c == 1)
+        def _():
+            partial_got[0] = total.astype(partial_got.dtype)
+
+        @pl.when(c == 0)
+        def _():
+            landed(partial_got.at[half], p_in.at[half])
+            whole = total + partial_got[half].astype(jnp.float32)
+            partial_got[0] = whole.astype(partial_got.dtype)
+
+        out = pltpu.make_async_copy(partial_got.at[0], grad_early, sums_in.at[0])
+        out.start()
+        out.wait()
 
     def taps_copies(fn_there, fn_here):
         def body(f, _):
@@ -484,6 +575,18 @@
 
         lax.fori_loop(0, n, body, 0)
 
+    def gather_sent(s, _):
+        @pl.when(other)
+        def _():
+            landed(own_slot(s, z, c), w_out.at[s])
+            upstream_copy(s).wait_send()
+
+        for k in range(depth - 1):
+            pl.when(jnp.logical_and(has_up, z - k >= 0))(lambda k=k: up(s, k).wait_send())
+            pl.when(jnp.logical_and(has_down, z + k < depth))(lambda k=k: down(s, k).wait_send())
+        lax.fori_loop(0, depth, lambda zz, _: (share(s, zz).wait_send(), 0)[1], 0)
+        return 0
+
     for i in range(2):
         sum_load(i).start()
 
@@ -496,9 +599,14 @@
         tokens_here(early_rows, early_in)
         conv_copy.wait_recv()
         taps_own[...] = jnp.zeros(taps_own.shape, jnp.float32)
-        wide = 2 * LANE
+        part_rows = min(rows, wide)
         for b in range(width // wide):
-            flipped[b * wide : (b + 1) * wide, :] = early_rows[:, b * wide : (b + 1) * wide].T
+            turned_block = early_rows[:, b * wide : (b + 1) * wide].T
+            for first in range(0, wide, part_rows):
+                f, at = divmod(b * wide + first, rows)
+                flipped[f % 2, pl.ds(f // 2 * rows + at, part_rows), :] = turned_block[
+                    first : first + part_rows
+                ]
 
     def delayed(t, at, steps, work):
         until = flush + at - last_hop
@@ -549,10 +657,17 @@
         guarded(t - lag, own_work)
         pl.when(t == lag)(third_wave)
 
-        @pl.when(t == strips + lag - 1)
-        def _():
+        @pl.when(t == ended)
+        def _():
+            conv_copy.wait_send()
+            for q in range(parts):
+                tokens_sent(early_copies[q])
+                tokens_sent(late_copies[q])
+            turned(early_rows, early_in, early_pass)
+            turned(late_rows, late_in, late_pass)
             taps_copies(lambda copy: copy.start(), lambda copy: copy.start())
             input_grad()
+            partial_start()
 
         for away in range(depth - 2, 0, -1):
             for upward in (True, False):
@@ -560,16 +675,23 @@
                 delayed(
                     t, lag + depth - 1 - away, DELAY * links, lambda s: pass_on(s, away, upward)
                 )
+        pl.when(t == ended + LATER)(partial_far)
+        for dx in range(1, half):
+            pl.when(t == ended + JOIN[0])(lambda: partial_joined(dx))
+        pl.when(t == ended + MEET)(partial_over)
+        pl.when(t == ended + JOIN[1])(lambda: partial_joined(0))
         links = jnp.maximum(jnp.where(has_down, z - 1, 0), jnp.where(has_up, depth - 2 - z, 0))
         delayed(t, last_hop + 1, DELAY * links, finish)
         delayed(t, last_hop + 2, DELAY * links, accept)
-        for i in range(tp_n):
-            pl.when(t == strips + lag - 1 + i // PER_STEP)(
-                lambda: partial_copy(tp_n - i, lambda copy: copy.start(), lambda copy: copy.start())
-            )
+
+        @pl.when(t == ended)
+        def _():
+            lax.fori_loop(0, strips, gather_sent, 0)
+
         return 0
 
-    lax.fori_loop(0, max(strips + lag + max(depth, tp_n), late_at + strips // 2 + 1), step, 0)
+    steps = max(ended + 1 + depth, ended + 1 + max(*JOIN, MEET, LATER), late_at + strips // 2 + 1)
+    lax.fori_loop(0, steps, step, 0)
 
     def taps_arrive(f, _):
         landed(taps_got.at[f], t_in.at[f])
@@ -581,22 +703,7 @@
         sum_of = sum_of + taps_got[i]
     new_taps[...] = sum_taps[...] + factor * sum_of[:taps_count]
 
-    for t in range(tp_n):
-        landed(partial_got.at[t], p_in.at[t])
-    total = partial_got[0].astype(jnp.float32)
-    for t in range(1, tp_n):
-        total = total + partial_got[t].astype(jnp.float32)
-    grad_early[...] = total.astype(grad_early.dtype)
-
-    conv_copy.wait_send()
-    for q in range(parts):
-        tokens_sent(early_copies[q])
-        tokens_sent(late_copies[q])
-    turned(early_rows, early_in, early_pass)
-    turned(late_rows, late_in, late_pass)
     taps_copies(lambda copy: copy.wait_send(), None)
-    for i in range(tp_n):
-        partial_copy(i, lambda copy: copy.wait_send(), None)
     for s in range(max(0, strips - 2), strips):
         to_partner(s).wait_send()
         hidden_sent(s)
@@ -607,21 +714,56 @@
 
         @pl.when(other)
         def _():
-            landed(own_slot(s, z, c), w_out.at[s])
-            upstream_copy(s).wait_send()
             hidden_copy(s, True).wait_recv()
             fin(s).wait_send()
 
-        for k in range(depth - 1):
-            pl.when(jnp.logical_and(has_up, z - k >= 0))(lambda k=k: up(s, k).wait_send())
-            pl.when(jnp.logical_and(has_down, z + k < depth))(lambda k=k: down(s, k).wait_send())
-            away = k + 1
+        for away in range(1, depth):
             pl.when(z + away < depth)(lambda away=away: along(s, z + away, away, True).wait_send())
             pl.when(z - away >= 0)(lambda away=away: along(s, z - away, away, False).wait_send())
-        lax.fori_loop(0, depth, lambda zz, _: (share(s, zz).wait_send(), 0)[1], 0)
         return 0
 
     lax.fori_loop(0, strips, drain, 0)
+    partial_total()
+    partial_sent()
+
+
+def out_kernel(halves, *refs):
+    count = len(halves)
+    sources, targets, held = refs[:count], refs[count : 2 * count], refs[2 * count : 3 * count]
+    in_sem, out_sem = refs[3 * count :]
+    copies = []
+    for i, cuts in enumerate(halves):
+        size = sources[i].shape[0] // cuts
+        for k in range(cuts):
+            at = pl.ds(k * size, size)
+            j = len(copies)
+            copies.append(
+                (
+                    pltpu.make_async_copy(sources[i].at[at], held[i].at[at], in_sem.at[j]),
+                    pltpu.make_async_copy(held[i].at[at], targets[i].at[at], out_sem.at[j]),
+                )
+            )
+    for there, _ in copies:
+        there.start()
+    for there, back in copies:
+        there.wait()
+        back.start()
+    for _, back in copies:
+        back.wait()
+
+
+def hand_out(results):
+    halves = tuple(2 if r.shape[0] % 32 == 0 else 1 for r in results)
+    hbm = pl.BlockSpec(memory_space=pl.ANY)
+    sems = pltpu.SemaphoreType.DMA((sum(halves),))
+    return pl.pallas_call(
+        functools.partial(out_kernel, halves),
+        out_shape=tuple(jax.ShapeDtypeStruct(r.shape, r.dtype) for r in results),
+        in_specs=[hbm] * len(results),
+        out_specs=(hbm,) * len(results),
+        scratch_shapes=[pltpu.VMEM(r.shape, r.dtype) for r in results] + [sems, sems],
+        name="hand_out",
+    )(*results)
 
 
 def shards(x_late, x_early, w_gate, w_value, conv_taps, grad_hidden, sum_gate, sum_value, sum_taps):
@@ -636,9 +778,9 @@
     vmem = pl.BlockSpec(memory_space=pltpu.VMEM)
     hbm = pl.BlockSpec(memory_space=pl.ANY)
     taps_shape = (8, columns)
-    hops = depth - 1
+    hops, half = depth - 1, tp_n // 2
     parts = next(q for q in (4, 2, 1) if piece % (16 * q) == 0)
-    return pl.pallas_call(
+    results = pl.pallas_call(
         functools.partial(kernel, n, tp_n, factor),
         out_shape=(
             jax.ShapeDtypeStruct((tokens, columns), bf16),
@@ -648,12 +790,12 @@
             jax.ShapeDtypeStruct(sum_taps.shape, f32),
         ),
         in_specs=[hbm] * 4 + [vmem] + [hbm] * 3 + [vmem],
-        out_specs=(hbm, vmem, hbm, hbm, vmem),
+        out_specs=(hbm,) * 4 + (vmem,),
         scratch_shapes=[
             pltpu.VMEM((strips, n * rows, 2 * LANE), bf16),
             pltpu.VMEM((tokens, width), bf16),
             pltpu.VMEM((tokens, width), bf16),
-            pltpu.VMEM((width, tokens), bf16),
+            pltpu.VMEM((2, width // 2, tokens), bf16),
             pltpu.VMEM((strips, tokens, 2 * LANE), bf16),
             pltpu.VMEM((strips, tokens, LANE), bf16),
             pltpu.VMEM((2, tokens, LANE), bf16),
@@ -662,14 +804,15 @@
             pltpu.VMEM((strips, hops, rows, 2 * LANE), bf16),
             pltpu.VMEM((strips, hops, rows, 2 * LANE), bf16),
             pltpu.VMEM((strips, rows, 2 * LANE), bf16),
-            pltpu.VMEM((tokens, width), bf16),
-            pltpu.VMEM((tp_n, piece, width), bf16),
+            pltpu.VMEM((half + 1, piece, width), bf16),
             pltpu.VMEM(taps_shape, f32),
             pltpu.VMEM((n,) + taps_shape, f32),
             pltpu.VMEM(conv_taps.shape, f32),
             pltpu.VMEM((tokens, width), f32),
             pltpu.VMEM((rows, columns), f32),
             pltpu.VMEM((rows, columns), f32),
+            pltpu.VMEM((max(half - 1, 1), piece, width), bf16),
+            pltpu.VMEM((half, piece, width), bf16),
         ]
         + [sems((strips,))] * 2
         + [sems((strips, hops))] * 4
@@ -683,7 +826,9 @@
         + [sems((tp_n,))] * 2
         + [sems((n,))] * 2
         + [sems, sems]
-        + [sems((2,)), sems((strips, 2))],
+        + [sems((2,)), sems((strips, 2))]
+        + [sems((max(half - 1, 1),))] * 2
+        + [sems((half,))] * 2,
         compiler_params=pltpu.CompilerParams(
             collective_id=0, has_side_effects=True, vmem_limit_bytes=67043328
         ),
@@ -691,6 +836,7 @@
     )(
         x_late, x_early, w_gate, w_value, conv_taps, grad_hidden, sum_gate, sum_value, sum_taps
     )
+    return hand_out(results)
 
 
 def solution(mesh):

time: 202 us -> 190 us (0.941)
  local copies, waits for them, and re-layouts: 8.42 us -> 0 us
  Pallas kernels: 193 us -> 189 us
    pallas_call x1, Pallas kernels: 193 us -> 184 us  [shards(): pl.pallas_call(functools.partial(kernel, n, tp_n, factor), out_shape=(jax...]
    unnamed x13 -> x0, local copies, waits for them, and re-layouts: 8.42 us -> none
    pallas_call x0 -> x1, Pallas kernels: none -> 4.9 us  [hand_out(): pl.pallas_call(functools.partial(out_kernel, halves), out_shape=tuple((ja...]
where the time goes in v3:
time: 190 us
  Pallas kernels  189 us (99%)
    pallas_call x1, Pallas kernels, shards(): pl.pallas_call(functools.partial(kernel, n, tp_n, factor), out_shape=(jax...  184 us
    pallas_call x1, Pallas kernels, hand_out(): pl.pallas_call(functools.partial(out_kernel, halves), out_shape=tuple((ja...  4.9 us

profile of v3, /device:TPU:1, one launch (start us, length us, event | category | flops | bytes accessed | tf_op | source)
XLA Modules:
  0.0 189.7 jit_solution(928056470380164279)
XLA Ops:
  0.6 184.1 %layer.1 = (bf16[768,1408]{1,0:T(8,128)(2,1)}, bf16[192,2048]{1,0:T(8,128)(2,1)}, f32[256,1408]{1,0:T(8,128)}, f32[256,1408]{1,0:T(8,128)}, f32[3,1408]{1,0:T(4,128)}) custom-call(bf16[192,2048]{1,0:T(8,128)(2,1)} %refs_0_.1, bf16[192,2048]{1,0:T(8,128)(2,1)} %refs_1_.1, bf16[256,1408]{1,0:T(8,128)(2,1)} %refs_2_.1, bf16[256,1408]{1,0:T(8,128)(2,1)} %refs_3_.1, ...), custom_call_target="tpu_custom_call" | custom-call | tf_op jit(solution)/shard_map/layer/pallas_call | solution.py:783
  184.8 4.9 %hand_out.1 = (bf16[768,1408]{1,0:T(8,128)(2,1)}, bf16[192,2048]{1,0:T(8,128)(2,1)}, f32[256,1408]{1,0:T(8,128)}, f32[256,1408]{1,0:T(8,128)}, f32[3,1408]{1,0:T(4,128)}) custom-call(bf16[768,1408]{1,0:T(8,128)(2,1)} %get-tuple-element.10.refs_0_, bf16[192,2048]{1,0:T(8,128)(2,1)} %get-tuple-element.11.refs_1_, f32[256,1408]{1,0:T(8,128)} %get-tuple-element.12.refs_2_, ...), custom_call_target="tpu_custom_call" | custom-call | tf_op jit(solution)/shard_map/hand_out/pallas_call | solution.py:759
